TPU v7x, 256 devices: a 4x2x16 block of a 4x16x16 slice. The times are simulated.
256 devices in a mesh: grp: 2 (over y), fs: 16 (over z), tp: 8 (over x, core).
Axes of the slice: x: 4, y: 2, z: 16, core: 2. Of those that a mesh axis runs over, the one named last changes fastest.
The devices are a block of a 4x16x16 slice.
Arguments:
- tokens: bfloat16 [32768, 2048], P(('grp', 'fs')), parts along dimension 0, may hold values from -1300 to 1300
- norm_gain: bfloat16 [2048], replicated, may hold values from 0.099609375 to 1.8984375
- gate_weight: bfloat16 [2048, 5120], P('fs', 'tp'), may hold values from -0.125 to 0.125
- up_weight: bfloat16 [2048, 5120], P('fs', 'tp'), may hold values from -0.125 to 0.125
- down_weight: bfloat16 [5120, 2048], P('tp', 'fs'), may hold values from -0.078125 to 0.078125
Outputs:
- mixed: bfloat16 [32768, 2048], P(('grp', 'fs', 'tp')), parts along dimension 0
There are 2 independent parts, one for each index of `grp`. A program takes and returns all parts, laid end to end along the dimension named above; an argument that names none is the same for every part. Nothing has to cross between parts.
All inputs are finite; a program needn't handle non-finite values.
Results may differ from a plain program's by a relative error of at most 0.013.
Values may be sent and summed in bfloat16 or wider, within the bound.
No kernel may reach another device: no remote copies, remote signals or barrier semaphores. Data moves between devices by JAX's collectives and lax.ppermute only.
A program may use at most 64 MiB of HBM per device.

v0:
```python
import jax
import jax.numpy as jnp
from jax import lax
from jax.sharding import PartitionSpec as P

EPSILON = 1e-06


def side_by_side(arrays, axis, dim, along):
    widths = [a.shape[along] for a in arrays]
    both = jnp.concatenate(arrays, axis=along)
    result = lax.all_gather(both, axis, axis=dim, tiled=True)
    return tuple(jnp.split(result, [sum(widths[:k]) for k in range(1, len(widths))], axis=along))


def normalize(tokens, norm_gain):
    as_float = tokens.astype(jnp.float32)
    scale = lax.rsqrt(jnp.mean(as_float * as_float, axis=-1, keepdims=True) + EPSILON)
    return (as_float * scale * norm_gain.astype(jnp.float32)).astype(jnp.bfloat16)


def rounded(values):
    return lax.optimization_barrier(values.astype(jnp.bfloat16)).astype(jnp.float32)


def on_device(tokens, norm_gain, gate_weight, up_weight, down_weight):
    normed = normalize(tokens, norm_gain)
    down_whole = lax.all_gather(down_weight, "fs", axis=1, tiled=True)
    gate_whole, up_whole = side_by_side((gate_weight, up_weight), "fs", 0, 1)
    gate_acts = jnp.dot(normed, gate_whole, preferred_element_type=jnp.float32)
    up_acts = jnp.dot(normed, up_whole, preferred_element_type=jnp.float32)
    hidden = (jax.nn.silu(gate_acts) * up_acts).astype(jnp.bfloat16)
    return lax.psum_scatter(
        rounded(jnp.dot(hidden, down_whole, preferred_element_type=jnp.float32)).astype(
            jnp.bfloat16
        ),
        "tp",
        scatter_dimension=0,
        tiled=True,
    )


def solution(mesh):
    return jax.shard_map(
        on_device,
        mesh=mesh,
        in_specs=(P(("grp", "fs"), None), P(), P("fs", "tp"), P("fs", "tp"), P("tp", "fs")),
        out_specs=P(("grp", "fs", "tp"), None),
        check_vma=False,
    )
```

profile of v0, /device:TPU:40, one launch (start us, length us, event | category | flops | bytes accessed | tf_op | source)
XLA Modules:
  0.0 240.0 jit_solution(12156880815646767167)
XLA Ops:
  6.5 0.0 all-gather.3.cloned.1.call-start
  6.6 1.7 pad_maximum_fusion
  8.3 0.1 all-gather.3.cloned.1.call-update
  8.4 0.1 all-gather.5.cloned.1.call-start
  8.4 0.7 all-gather.5.cloned.1.call-update
  9.2 0.1 reduce-scatter.2.cloned.1.call-start
  9.2 0.7 convert_element_type.18
  9.9 3.1 %fusion = f32[1024]{0:T(1024)S(1)} fusion(bf16[1024,2048]{1,0:T(8,128)(2,1)} %param.5), kind=kLoop, calls=%fused_computation.2 | loop fusion | flops 6290432 | bytes 4198400 | tf_op jit(solution)/shard_map/reduce_sum | solution.py:18
  13.0 88.4 %all-gather.3.cloned.1.call-done = bf16[2048,1280]{1,0:T(8,128)(2,1)} async-done(((bf16[128,1280]{1,0:T(8,128)(2,1)}), bf16[2048,1280]{1,0:T(8,128)(2,1)}) %all-gather.3.cloned.1.call-update) | async-done | bytes 5242896 | tf_op jit(solution)/shard_map/all_gather | solution.py:12
  101.4 6.3 %fusion.3 = f32[1024,640]{1,0:T(8,128)S(1)} fusion(bf16[2048,1280]{1,0:T(8,128)(2,1)} %all-gather.3.cloned.1.call-done, bf16[1024,2048]{1,0:T(8,128)(2,1)} %param.5, f32[2048]{0:T(1024)S(1)} %convert_element_type.18, f32[1024]{0:T(1024)S(1)} %add_rsqrt_fusion), kind=kOutput, calls=%fused_computation.6 | convolution fusion | flops 2692743168 | bytes 9449472 | tf_op jit(solution)/shard_map/dot_general | solution.py:31
  107.7 72.3 %all-gather.5.cloned.1.call-done = bf16[640,2048]{1,0:T(8,128)(2,1)} async-done(((bf16[640,128]{1,0:T(8,128)(2,1)}), bf16[640,2048]{1,0:T(8,128)(2,1)}) %all-gather.5.cloned.1.call-update) | async-done | bytes 2621456 | tf_op jit(solution)/shard_map/all_gather | solution.py:28
  180.0 12.9 %convolution_convert_fusion = bf16[1024,2048]{1,0:T(8,128)(2,1)} fusion(bf16[640,2048]{1,0:T(8,128)(2,1)} %all-gather.5.cloned.1.call-done, f32[1024,640]{1,0:T(8,128)S(1)} %fusion.3, bf16[2048,1280]{1,0:T(8,128)(2,1)} %all-gather.3.cloned.1.call-done, bf16[1024,2048]{1,0:T(8,128)(2,1)} %param.5, f32[2048]{0:T(1024)S(1)} %convert_element_type.18, ...), kind=kOutput, calls=%fused_computation.5 | convolution fusion | flops 5383127040 | bytes 16265216 | tf_op jit(solution)/shard_map/dot_general | solution.py:34
  192.9 0.1 reduce-scatter.2.cloned.1.call-update
  192.9 40.5 %reduce-scatter.2.cloned.1.call-done = bf16[128,2048]{1,0:T(8,128)(2,1)} async-done(((bf16[1024,2048]{1,0:T(8,128)(2,1)}), bf16[128,2048]{1,0:T(8,128)(2,1)}) %reduce-scatter.2.cloned.1.call-update) | async-done | bytes 524304 | tf_op jit(solution)/shard_map/reduce_scatter | solution.py:33
  (1 shorter events, 0.0 us)
Async XLA Ops:
  6.5 94.9 %all-gather.3.cloned.1.call-start = ((), (), s32[]{:S(2)}) async-start(), calls=%async_computation.1 | async-start | bytes 5570560 | tf_op jit(solution)/shard_map/all_gather | solution.py:12
  8.4 171.7 %all-gather.5.cloned.1.call-start = ((), (), s32[]{:S(2)}) async-start(), calls=%async_computation.2 | async-start | bytes 2785280 | tf_op jit(solution)/shard_map/all_gather | solution.py:28
  9.2 224.2 %reduce-scatter.2.cloned.1.call-start = ((), (), s32[]{:S(2)}) async-start(), calls=%async_computation.3 | async-start | bytes 4718592 | tf_op jit(solution)/shard_map/reduce_scatter | solution.py:33
Sparse Core Ops, SparseCore 0:
  9.1 92.2 all-gather.2
  103.2 76.7 all-gather.4
  193.0 40.3 reduce-scatter.1
where the time goes:
time: 240 us
  waiting for transfers between devices  202 us (84%)
  matrix products  19.1 us (8%)
  between operations  13.1 us (5%)
  other arithmetic  5.51 us (2%)
    all_gather x1, waiting for transfers between devices, side_by_side(): result = lax.all_gather(both, axis, axis=dim, tiled=True)  88.4 us
    all_gather x1, waiting for transfers between devices, on_device(): down_whole = lax.all_gather(down_weight, 'fs', axis=1, tiled=True)  72.3 us
    reduce_scatter x1, waiting for transfers between devices, on_device(): lax.psum_scatter(rounded(jnp.dot(hidden, down_whole, preferred_element_ty...  40.5 us
    dot_general x1, matrix products, on_device(): jnp.dot(hidden, down_whole, preferred_element_type=jnp.float32)  12.9 us
    dot_general x1, matrix products, on_device(): up_acts = jnp.dot(normed, up_whole, preferred_element_type=jnp.float32)  6.29 us
  transfers between devices with their start and end apart: 3, of which 3 were waited for; matrix products, arithmetic and copies ran while one was open for 4% of the time, Pallas kernels for 0%

commit v1 on v0

v1 whole, which is shorter than its diff:
```python
import functools

import jax
import jax.numpy as jnp
from jax import lax
from jax.experimental import pallas as pl
from jax.experimental.pallas import tpu as pltpu
from jax.sharding import PartitionSpec as P


EPSILON = 1e-06
B = 128
F32 = jnp.float32
BF16 = jnp.bfloat16


def hbm(v):
    return pltpu.with_memory_space_constraint(v, pltpu.HBM)


def vmem(mb):
    return pltpu.CompilerParams(vmem_limit_bytes=mb * 1024 * 1024)


def on_chip(n):
    return [pl.BlockSpec(memory_space=pltpu.VMEM)] * n


RING_BLOCKS = (("g", 0), ("g", 1), ("u", 0), ("u", 1), ("d", 0), ("g", 2), ("u", 2), ("d", 1), ("d", 2), ("d", 3))
PAIR_BLOCKS = (("g", 4), ("g", 3), ("u", 4), ("u", 3), ("d", 4))
SHARED = 5
SLOTS = 5


def pack(meta, gate, up, down):
    def body(m, g, u, d, zo, yo):
        def put(flip):
            for out, names in ((zo, RING_BLOCKS), (yo, PAIR_BLOCKS)):
                for n, (what, k) in enumerate(names):
                    c = slice((SLOTS - 1 - k if flip else k) * B, (SLOTS - k if flip else k + 1) * B)
                    out[n] = d[c, :] if what == "d" else (g if what == "g" else u)[:, c]

        pl.when(m[3] == 0)(lambda: put(False))
        pl.when(m[3] != 0)(lambda: put(True))

    whole = lambda v: pl.BlockSpec(v.shape, lambda i, m: (0, 0))
    return pl.pallas_call(
        body,
        grid_spec=pltpu.PrefetchScalarGridSpec(
            num_scalar_prefetch=1, grid=(1,), in_specs=[whole(gate), whole(up), whole(down)], out_specs=on_chip(2)
        ),
        out_shape=[pltpu.VMEM((len(RING_BLOCKS), B, B), gate.dtype), pltpu.VMEM((len(PAIR_BLOCKS), B, B), gate.dtype)],
        compiler_params=vmem(4),
    )(meta, hbm(gate), hbm(up), hbm(down))


def normalize(tokens, gain, meta, ring):
    rows, width = tokens.shape
    tile, step = 256, 16

    def body(m, t, g, out):
        z = m[2]

        def chunk(n, _):
            x = t[pl.ds(pl.multiple_of(n * step, step), step), :].astype(F32)
            scale = lax.rsqrt(jnp.mean(x * x, axis=-1, keepdims=True) + EPSILON)
            y = (x * scale * g[...].astype(F32)).astype(BF16)
            at = pl.ds(pl.multiple_of(pl.program_id(0) * tile + n * step, step), step)
            for b in range(ring):
                i = lax.rem(b - z + ring + ring // 2, ring)
                out[at, pl.ds(pl.multiple_of(i * B, B), B)] = y[:, b * B:(b + 1) * B]
            return 0

        lax.fori_loop(0, tile // step, chunk, 0, unroll=2)

    return pl.pallas_call(
        body,
        grid_spec=pltpu.PrefetchScalarGridSpec(
            num_scalar_prefetch=1,
            grid=(rows // tile,),
            in_specs=[pl.BlockSpec((tile, width), lambda i, m: (i, 0)), pl.BlockSpec((1, width), lambda i, m: (0, 0))],
            out_specs=on_chip(1)[0],
        ),
        out_shape=pltpu.VMEM((rows, width), BF16),
        compiler_params=vmem(8),
        cost_estimate=pl.CostEstimate(flops=rows * width * 16, bytes_accessed=rows * width * 4, transcendentals=0),
    )(meta, hbm(tokens), gain.reshape(1, width))


class Parts:
    def __init__(self, pieces, ids):
        self.args, self.where = [], {}
        for i in ids:
            for array, lo, names in pieces[i]:
                n = next((n for n, v in enumerate(self.args) if v is array), len(self.args))
                if n == len(self.args):
                    self.args.append(array)
                for j, name in enumerate(names):
                    self.where[i, name] = (n, lo + j)

    def block(self, refs, i, name):
        n, j = self.where[i, name]
        return refs[n][j]

    def gate_up(self, refs, ids, k):
        rows = [jnp.concatenate([self.block(refs, i, ("g", k)), self.block(refs, i, ("u", k))], axis=1) for i in ids]
        return jnp.concatenate(rows, axis=0)

    def down(self, refs, ids):
        cols = [jnp.concatenate([self.block(refs, i, ("d", k)) for k in range(SLOTS)], axis=0) for i in ids]
        return jnp.concatenate(cols, axis=1)


def runs(ids):
    out = []
    for i in ids:
        if out and out[-1][1] == i:
            out[-1][1] = i + 1
        else:
            out.append([i, i + 1])
    return out


def take(ref, rows, ids):
    cols = [ref[rows, a * B:b * B] for a, b in runs(ids)]
    return cols[0] if len(cols) == 1 else jnp.concatenate(cols, axis=1)


def accumulate(normed, ids, pieces, acc):
    rows = normed.shape[0]
    tile = 512
    gu = Parts(pieces, ids)
    old = [] if acc is None else [acc]

    def body(x, *rest):
        refs, out = rest[len(old):-1], rest[-1]
        for k in range(SLOTS):
            w = gu.gate_up(refs, ids, k)
            c = slice(2 * k * B, 2 * (k + 1) * B)
            for r in range(0, rows, tile):
                at = slice(r, r + tile)
                part = jnp.dot(take(x, at, ids), w, preferred_element_type=F32)
                out[at, c] = rest[0][at, c] + part if old else part

    return pl.pallas_call(
        body,
        in_specs=on_chip(1 + len(old) + len(gu.args)),
        out_specs=on_chip(1)[0],
        out_shape=pltpu.VMEM((rows, 2 * SLOTS * B), F32),
        input_output_aliases={1: 0} if old else {},
        compiler_params=vmem(6),
        cost_estimate=pl.CostEstimate(flops=4 * rows * len(ids) * B * SLOTS * B, bytes_accessed=rows * SLOTS * B * 16, transcendentals=0),
    )(normed, *old, *gu.args)


def finish(meta, normed, ids, pieces, acc, rel):
    rows = normed.shape[0]
    chips = rows // (2 * B)
    ring = len(pieces)
    parts = Parts(pieces, range(ring))

    def body(m, x, a, *rest):
        refs, (keep, send) = rest[:-2], rest[-2:]
        chip = lax.rem(m[0] + rel, chips)
        mine = pl.ds(pl.multiple_of((2 * chip + m[1]) * B, B), B)
        theirs = pl.ds(pl.multiple_of((2 * chip + 1 - m[1]) * B, B), B)
        v = jnp.concatenate([take(x, mine, ids), take(x, theirs, ids)], axis=0)
        h = []
        for k in range(SLOTS):
            c = slice(2 * k * B, 2 * (k + 1) * B)
            act = jnp.concatenate([a[mine, c], a[theirs, c]], axis=0)
            act = act + jnp.dot(v, parts.gate_up(refs, ids, k), preferred_element_type=F32)
            gate = act[:, :B]
            h.append((gate / (1.0 + jnp.exp(-gate)) * act[:, B:]).astype(BF16))
        h = jnp.concatenate(h, axis=1)
        for j in range(0, ring, 2):
            c = slice(j * B, (j + 2) * B)
            y = jnp.dot(h, parts.down(refs, [j, j + 1]), preferred_element_type=F32).astype(BF16)
            keep[:, c] = y[:B]
            send[:, c] = y[B:]

    half = pltpu.VMEM((B, ring * B), BF16)
    return pl.pallas_call(
        body,
        in_specs=[pl.BlockSpec(memory_space=pltpu.SMEM)] + on_chip(2 + len(parts.args)),
        out_specs=on_chip(2),
        out_shape=[half, half],
        compiler_params=vmem(6),
        cost_estimate=pl.CostEstimate(flops=4 * B * SLOTS * B * (2 * len(ids) * B + ring * B), bytes_accessed=8 << 20, transcendentals=2 * B * SLOTS * B),
    )(meta, normed, acc, *parts.args)


def both(a, b):
    return a[...].astype(F32) + b[...].astype(F32)


def far(keep, got):
    rows, cols = keep.shape
    h = rows // 2

    def body(k, g, a, b):
        v = both(k, g).astype(BF16)
        a[...] = v[:h]
        b[...] = v[h:]

    out = jax.ShapeDtypeStruct((h, cols), BF16)
    return pl.pallas_call(body, out_shape=[out, out], compiler_params=vmem(8))(keep, got)


def near(keep1, got1, keep3, got3, more):
    rows, cols = keep1.shape
    h = rows // 2

    def body(k1, g1, k3, g3, *rest):
        o1, o3 = rest[-2:]
        if more:
            o1[...] = (both(k1, g1) + rest[0][...].astype(F32)).astype(BF16)
            o3[...] = (both(k3, g3) + rest[1][...].astype(F32)).astype(BF16)
        else:
            o1[...] = both(k1, g1).astype(BF16)
            o3[...] = both(k3, g3).astype(BF16)

    top = pl.BlockSpec((h, cols), lambda i: (0, 0))
    low = pl.BlockSpec((h, cols), lambda i: (1, 0))
    first = [top, top, low, low] if more else [low, low, top, top]
    out = jax.ShapeDtypeStruct((h, cols), BF16)
    return pl.pallas_call(
        body, grid=(1,), in_specs=first + [top] * len(more), out_specs=[top, top], out_shape=[out, out], compiler_params=vmem(8)
    )(keep1, got1, keep3, got3, *more)


def total(meta, keep, got, free1, rest1, free3, rest3, ring):
    rows, cols = keep.shape
    h = rows // 2

    def body(m, k, g, f1, r1, f3, r3, out):
        top = (both(k.at[:h], g.at[:h]) + both(r1, f3)).astype(BF16)
        low = (both(k.at[h:], g.at[h:]) + both(f1, r3)).astype(BF16)
        for j in range(ring):
            at = pl.ds(pl.multiple_of(lax.rem(j + m[2] + ring // 2, ring) * B, B), B)
            out[:h, at] = top[:, j * B:(j + 1) * B]
            out[h:, at] = low[:, j * B:(j + 1) * B]

    full = pl.BlockSpec((rows, cols), lambda i, m: (0, 0))
    part = pl.BlockSpec((h, cols), lambda i, m: (0, 0))
    return pl.pallas_call(
        body,
        grid_spec=pltpu.PrefetchScalarGridSpec(num_scalar_prefetch=1, grid=(1,), in_specs=[full, full, part, part, part, part], out_specs=full),
        out_shape=jax.ShapeDtypeStruct((rows, cols), BF16),
        compiler_params=vmem(8),
    )(meta, keep, got, free1, rest1, free3, rest3)


def on_device(sizes, tokens, norm_gain, gate_weight, up_weight, down_weight):
    ring, tp, groups = sizes["fs"], sizes["tp"], sizes["grp"]
    half = ring // 2

    def shift(v, k):
        return lax.ppermute(v, "fs", [(i, (i + k) % ring) for i in range(ring)])

    def chip(v, k):
        return lax.ppermute(v, "tp", [(i, (i + 2 * k) % tp) for i in range(tp)])

    def core(v):
        return lax.ppermute(v, "tp", [(i, i ^ 1) for i in range(tp)])

    def pair(v):
        return lax.ppermute(v, "grp", [(i, i ^ 1) for i in range(groups)])

    t = lax.axis_index("tp")
    meta = jnp.stack([t // 2, t % 2, lax.axis_index("fs"), lax.axis_index("grp") % 2]).astype(jnp.int32)

    f, own = pack(meta, gate_weight, up_weight, down_weight)
    pieces = {half: [(f, 0, RING_BLOCKS), (own, 0, PAIR_BLOCKS)]}
    g = f
    for s in range(1, half):
        f = shift(f, 1)
        g = shift(g, -1)
        y = jnp.concatenate([f[:SHARED], g[:SHARED]])
        y = pair(y)
        pieces[half - s] = [(f, 0, RING_BLOCKS), (y, 0, PAIR_BLOCKS)]
        pieces[half + s] = [(g, 0, RING_BLOCKS), (y, SHARED, PAIR_BLOCKS)]
    f = shift(f[:SHARED], 1)
    g = shift(g[SHARED:], -1)
    y = pair(f)
    pieces[0] = [(f, 0, RING_BLOCKS[:SHARED]), (g, 0, RING_BLOCKS[SHARED:]), (y, 0, PAIR_BLOCKS)]
    normed = normalize(tokens, norm_gain, meta, ring)
    acc = accumulate(normed, list(range(half - 3, half + 4)), pieces, None)
    acc = accumulate(normed, [2, 3, 4, ring - 4, ring - 3, ring - 2], pieces, acc)
    last = [0, 1, ring - 1]
    done = {}
    for rel in (2, 1, 3, 0):
        keep, send = finish(meta, normed, last, pieces, acc, rel)
        done[rel] = (keep, core(send))
    a, b = far(*done[2])
    a, b = chip(a, 1), chip(b, -1)
    f1, f3 = near(*done[1], *done[3], ())
    f1, f3 = chip(f1, 1), chip(f3, -1)
    r1, r3 = near(*done[1], *done[3], (a, b))
    r1, r3 = chip(r1, 1), chip(r3, -1)
    return total(meta, *done[0], f1, r1, f3, r3, ring)


def solution(mesh):
    spec = P(("grp", "fs"), None)
    return jax.shard_map(
        functools.partial(on_device, dict(mesh.shape)),
        mesh=mesh,
        in_specs=(spec, P(), P("fs", "tp"), P("fs", "tp"), P("tp", "fs")),
        out_specs=P(("grp", "fs", "tp"), None),
        check_vma=False,
    )
```

time: 240 us -> 158 us (0.66)
  waiting for transfers between devices: 202 us -> 72.9 us
  starting transfers between devices: 0.13 us -> 58.9 us
  Pallas kernels: 0 us -> 23.4 us
  matrix products: 19.1 us -> 0 us
  between operations: 13.1 us -> 0.33 us
  other arithmetic: 5.51 us -> 0.3 us
    all_gather x2 -> x0, waiting for transfers between devices: 161 us -> none  [the longest x1 88.4 us: side_by_side(): result = lax.all_gather(both, axis, axis=dim, tiled=True)]
    ppermute x0 -> x34, waiting for transfers between devices: none -> 72.9 us  [the longest x16 39.1 us: shift(): return lax.ppermute(v, 'fs', [(i, (i + k) % ring) for i in range(ring)])]
    ppermute x0 -> x34, starting transfers between devices: none -> 58.9 us  [the longest x16 42.7 us: shift(): return lax.ppermute(v, 'fs', [(i, (i + k) % ring) for i in range(ring)])]
    reduce_scatter x1 -> x0, waiting for transfers between devices: 40.5 us -> none  [on_device(): lax.psum_scatter(rounded(jnp.dot(hidden, down_whole, preferred_element_ty...]
    pallas_call x0 -> x12, Pallas kernels: none -> 23.4 us  [the longest x4 7.64 us: finish(): pl.pallas_call(body, in_specs=[pl.BlockSpec(memory_space=pltpu.SMEM)] + o...]
    dot_general x2 -> x0, matrix products: 19.1 us -> none  [the longest x1 12.9 us: on_device(): jnp.dot(hidden, down_whole, preferred_element_type=jnp.float32)]
    reduce_sum x1 -> x0, other arithmetic: 3.07 us -> none  [normalize(): jnp.mean(as_float * as_float, axis=-1, keepdims=True) + EPSILON]
  transfers between devices with their start and end apart: 3 -> 34, of which waited for: 3 -> 17; matrix products, arithmetic and copies ran while one was open for 4% -> 1% of each run, Pallas kernels for 0% -> 12%
where the time goes in v1:
time: 158 us; the launch traced here: 157 us
  waiting for transfers between devices  72.9 us (46%)
  starting transfers between devices  58.9 us (37%)
  Pallas kernels  23.4 us (15%)
    ppermute x16, starting transfers between devices, shift(): return lax.ppermute(v, 'fs', [(i, (i + k) % ring) for i in range(ring)])  42.7 us
    ppermute x16, waiting for transfers between devices, shift(): return lax.ppermute(v, 'fs', [(i, (i + k) % ring) for i in range(ring)])  39.1 us
    ppermute x8, waiting for transfers between devices, pair(): return lax.ppermute(v, 'grp', [(i, i ^ 1) for i in range(groups)])  23.1 us
    ppermute x6, waiting for transfers between devices, chip(): return lax.ppermute(v, 'tp', [(i, (i + 2 * k) % tp) for i in range(tp)])  10.8 us
    ppermute x6, starting transfers between devices, chip(): return lax.ppermute(v, 'tp', [(i, (i + 2 * k) % tp) for i in range(tp)])  10.1 us
    pallas_call x4, Pallas kernels, finish(): pl.pallas_call(body, in_specs=[pl.BlockSpec(memory_space=pltpu.SMEM)] + o...  7.64 us
    pallas_call x1, Pallas kernels, normalize(): pl.pallas_call(body, grid_spec=pltpu.PrefetchScalarGridSpec(num_scalar_pr...  6.37 us
    pallas_call x2, Pallas kernels, accumulate(): pl.pallas_call(body, in_specs=on_chip(1 + len(old) + len(gu.args)), out_s...  5.63 us
  transfers between devices with their start and end apart: 34, of which 17 were waited for; matrix products, arithmetic and copies ran while one was open for 1% of the time, Pallas kernels for 12%

profile of v1, /device:TPU:40, one launch (start us, length us, event | category | flops | bytes accessed | tf_op | source)
XLA Modules:
  0.0 156.7 jit_solution(13734183436314417683)
XLA Ops:
  0.0 0.1 pad_add_fusion.m
  0.1 1.7 %shard_map.56 = (bf16[10,128,128]{2,1,0:T(8,128)(2,1)S(1)}, bf16[5,128,128]{2,1,0:T(8,128)(2,1)S(1)}) custom-call(s32[4]{0:T(128)S(1)} %pad_add_fusion.m, bf16[128,640]{1,0:T(8,128)(2,1)} %g.1, bf16[128,640]{1,0:T(8,128)(2,1)} %u.1, bf16[640,128]{1,0:T(8,128)(2,1)} %d.1), custom_call_target="tpu_custom_call" | custom-call | tf_op jit(solution)/shard_map/pallas_call | solution.py:47
  1.8 2.9 %collective-permute-start = (bf16[10,128,128]{2,1,0:T(8,128)(2,1)S(1)}, bf16[10,128,128]{2,1,0:T(8,128)(2,1)S(1)}, u32[]{:S(2)}, u32[]{:S(2)}) collective-permute-start(bf16[10,128,128]{2,1,0:T(8,128)(2,1)S(1)} %get-tuple-element.21.rest_6_.rest_17_), channel_id=1, source_target_pairs={{0,8},{8,16},{16,24},{24,32},{32,40},{40,48},{48,56},{56,64},{64,7... | collective-permute-start | bytes 983048 | tf_op jit(solution)/shard_map/ppermute | solution.py:259
  4.7 19.7 %collective-permute-start.3 = (bf16[10,128,128]{2,1,0:T(8,128)(2,1)S(1)}, bf16[10,128,128]{2,1,0:T(8,128)(2,1)S(1)}, u32[]{:S(2)}, u32[]{:S(2)}) collective-permute-start(bf16[10,128,128]{2,1,0:T(8,128)(2,1)S(1)} %get-tuple-element.21.rest_6_.rest_17_), channel_id=1, source_target_pairs={{0,120},{8,0},{16,8},{24,16},{32,24},{40,32},{48,40},{56,48},{64,5... | collective-permute-start | bytes 983048 | tf_op jit(solution)/shard_map/ppermute | solution.py:259
  24.4 7.7 %collective-permute-done.rest_4_.rest_15_ = bf16[10,128,128]{2,1,0:T(8,128)(2,1)S(1)} collective-permute-done((bf16[10,128,128]{2,1,0:T(8,128)(2,1)S(1)}, bf16[10,128,128]{2,1,0:T(8,128)(2,1)S(1)}, u32[]{:S(2)}, u32[]{:S(2)}) %collective-permute-start) | collective-permute-done | bytes 327712 | tf_op jit(solution)/shard_map/ppermute | solution.py:259
  32.0 0.0 collective-permute-start.1
  32.0 0.0 collective-permute-done.3.rest_8_.rest_19_
  32.1 3.2 %collective-permute-start.4 = (bf16[10,128,128]{2,1,0:T(8,128)(2,1)S(1)}, bf16[10,128,128]{2,1,0:T(8,128)(2,1)S(1)}, u32[]{:S(2)}, u32[]{:S(2)}) collective-permute-start(bf16[10,128,128]{2,1,0:T(8,128)(2,1)S(1)} %collective-permute-done.3.rest_8_.rest_19_), channel_id=1, source_target_pairs={{0,120},{8,0},{16,8},{24,16},{32,24},{40,32},{48,40},{56,48},{64,5... | collective-permute-start | bytes 983048 | tf_op jit(solution)/shard_map/ppermute | solution.py:259
  35.3 6.9 %collective-permute-done.1.rest_2_.rest_13_ = bf16[10,128,128]{2,1,0:T(8,128)(2,1)S(1)} collective-permute-done((bf16[10,128,128]{2,1,0:T(8,128)(2,1)S(1)}, bf16[10,128,128]{2,1,0:T(8,128)(2,1)S(1)}, u32[]{:S(2)}, u32[]{:S(2)}) %collective-permute-start.1) | collective-permute-done | bytes 327712 | tf_op jit(solution)/shard_map/ppermute | solution.py:259
  42.2 0.0 collective-permute-start.2
  42.2 0.0 collective-permute-done.4.rest_9_.rest_20_
  42.2 3.2 %collective-permute-start.5 = (bf16[10,128,128]{2,1,0:T(8,128)(2,1)S(1)}, bf16[10,128,128]{2,1,0:T(8,128)(2,1)S(1)}, u32[]{:S(2)}, u32[]{:S(2)}) collective-permute-start(bf16[10,128,128]{2,1,0:T(8,128)(2,1)S(1)} %collective-permute-done.4.rest_9_.rest_20_), channel_id=1, source_target_pairs={{0,120},{8,0},{16,8},{24,16},{32,24},{40,32},{48,40},{56,48},{64,5... | collective-permute-start | bytes 983048 | tf_op jit(solution)/shard_map/ppermute | solution.py:259
  45.4 6.1 %collective-permute-done.2.rest_0_.rest_11_ = bf16[10,128,128]{2,1,0:T(8,128)(2,1)S(1)} collective-permute-done((bf16[10,128,128]{2,1,0:T(8,128)(2,1)S(1)}, bf16[10,128,128]{2,1,0:T(8,128)(2,1)S(1)}, u32[]{:S(2)}, u32[]{:S(2)}) %collective-permute-start.2) | collective-permute-done | bytes 327712 | tf_op jit(solution)/shard_map/ppermute | solution.py:259
  51.5 0.0 collective-permute-start.9
  51.5 3.2 %collective-permute-start.12 = (bf16[10,128,128]{2,1,0:T(8,128)(2,1)S(1)}, bf16[10,128,128]{2,1,0:T(8,128)(2,1)S(1)}, u32[]{:S(2)}, u32[]{:S(2)}) collective-permute-start(bf16[10,128,128]{2,1,0:T(8,128)(2,1)S(1)} %collective-permute-done.5.rest_10_.rest_21_), channel_id=1, source_target_pairs={{0,120},{8,0},{16,8},{24,16},{32,24},{40,32},{48,40},{56,48},{64,5... | collective-permute-start | bytes 983048 | tf_op jit(solution)/shard_map/ppermute | solution.py:259
  54.7 5.2 %collective-permute-done.9.rest_5_.rest_9_ = bf16[10,128,128]{2,1,0:T(8,128)(2,1)S(1)} collective-permute-done((bf16[10,128,128]{2,1,0:T(8,128)(2,1)S(1)}, bf16[10,128,128]{2,1,0:T(8,128)(2,1)S(1)}, u32[]{:S(2)}, u32[]{:S(2)}) %collective-permute-start.9) | collective-permute-done | bytes 327712 | tf_op jit(solution)/shard_map/ppermute | solution.py:259
  59.9 0.0 collective-permute-start.10
  59.9 3.2 %collective-permute-start.13 = (bf16[10,128,128]{2,1,0:T(8,128)(2,1)S(1)}, bf16[10,128,128]{2,1,0:T(8,128)(2,1)S(1)}, u32[]{:S(2)}, u32[]{:S(2)}) collective-permute-start(bf16[10,128,128]{2,1,0:T(8,128)(2,1)S(1)} %collective-permute-done.12.rest_7_.rest_22_), channel_id=1, source_target_pairs={{0,120},{8,0},{16,8},{24,16},{32,24},{40,32},{48,40},{56,48},{64,5... | collective-permute-start | bytes 983048 | tf_op jit(solution)/shard_map/ppermute | solution.py:259
  63.2 0.7 reshape.3.g
  63.9 6.4 %shard_map.55.x = bf16[1024,2048]{1,0:T(8,128)(2,1)S(1)} custom-call(s32[4]{0:T(128)S(1)} %pad_add_fusion.m, bf16[1024,2048]{1,0:T(8,128)(2,1)} %t.1, bf16[1,2048]{1,0:T(2,128)(2,1)S(1)} %reshape.3.g), custom_call_target="tpu_custom_call" | custom-call | flops 33554432 | bytes 8388608 | tf_op jit(solution)/shard_map/pallas_call | solution.py:76
  70.3 0.1 collective-permute-start.11
  70.4 3.2 %collective-permute-start.14 = (bf16[10,128,128]{2,1,0:T(8,128)(2,1)S(1)}, bf16[10,128,128]{2,1,0:T(8,128)(2,1)S(1)}, u32[]{:S(2)}, u32[]{:S(2)}) collective-permute-start(bf16[10,128,128]{2,1,0:T(8,128)(2,1)S(1)} %collective-permute-done.13.rest_8_.rest_23_), channel_id=1, source_target_pairs={{0,120},{8,0},{16,8},{24,16},{32,24},{40,32},{48,40},{56,48},{64,5... | collective-permute-start | bytes 983048 | tf_op jit(solution)/shard_map/ppermute | solution.py:259
  73.7 0.1 collective-permute-start.8
  73.9 2.1 %collective-permute-start.7 = (bf16[10,128,128]{2,1,0:T(8,128)(2,1)S(1)}, bf16[10,128,128]{2,1,0:T(8,128)(2,1)S(1)}, u32[]{:S(2)}, u32[]{:S(2)}) collective-permute-start(bf16[10,128,128]{2,1,0:T(8,128)(2,1)S(1)} %pad_maximum_fusion.1), channel_id=1, source_target_pairs={{0,128},{128,0},{1,129},{129,1},{2,130},{130,2},{3,131},{131,3},{4... | collective-permute-start | bytes 983048 | tf_op jit(solution)/shard_map/ppermute | solution.py:268
  76.1 0.2 collective-permute-start.6
  76.3 3.4 %collective-permute-done.14.rest_9_.rest_24_ = bf16[10,128,128]{2,1,0:T(8,128)(2,1)S(1)} collective-permute-done((bf16[10,128,128]{2,1,0:T(8,128)(2,1)S(1)}, bf16[10,128,128]{2,1,0:T(8,128)(2,1)S(1)}, u32[]{:S(2)}, u32[]{:S(2)}) %collective-permute-start.14) | collective-permute-done | bytes 327712 | tf_op jit(solution)/shard_map/ppermute | solution.py:259
  79.7 3.7 %collective-permute-start.20 = (bf16[10,128,128]{2,1,0:T(8,128)(2,1)S(1)}, bf16[10,128,128]{2,1,0:T(8,128)(2,1)S(1)}, u32[]{:S(2)}, u32[]{:S(2)}) collective-permute-start(bf16[10,128,128]{2,1,0:T(8,128)(2,1)S(1)} %collective-permute-done.14.rest_9_.rest_24_), channel_id=1, source_target_pairs={{0,120},{8,0},{16,8},{24,16},{32,24},{40,32},{48,40},{56,48},{64,5... | collective-permute-start | bytes 983048 | tf_op jit(solution)/shard_map/ppermute | solution.py:259
  83.6 9.8 %collective-permute-done.18.rest_3_ = bf16[10,128,128]{2,1,0:T(8,128)(2,1)S(1)} collective-permute-done((bf16[10,128,128]{2,1,0:T(8,128)(2,1)S(1)}, bf16[10,128,128]{2,1,0:T(8,128)(2,1)S(1)}, u32[]{:S(2)}, u32[]{:S(2)}) %collective-permute-start.18) | collective-permute-done | bytes 327712 | tf_op jit(solution)/shard_map/ppermute | solution.py:259
  93.4 2.1 %collective-permute-start.16 = (bf16[10,128,128]{2,1,0:T(8,128)(2,1)S(1)}, bf16[10,128,128]{2,1,0:T(8,128)(2,1)S(1)}, u32[]{:S(2)}, u32[]{:S(2)}) collective-permute-start(bf16[10,128,128]{2,1,0:T(8,128)(2,1)S(1)} %pad_maximum_fusion.4), channel_id=1, source_target_pairs={{0,128},{128,0},{1,129},{129,1},{2,130},{130,2},{3,131},{131,3},{4... | collective-permute-start | bytes 983048 | tf_op jit(solution)/shard_map/ppermute | solution.py:268
  95.6 0.2 collective-permute-start.15
  95.8 0.1 collective-permute-start.19
  96.0 2.5 %collective-permute-done.6.rest_1_.rest_12_ = bf16[10,128,128]{2,1,0:T(8,128)(2,1)S(1)} collective-permute-done((bf16[10,128,128]{2,1,0:T(8,128)(2,1)S(1)}, bf16[10,128,128]{2,1,0:T(8,128)(2,1)S(1)}, u32[]{:S(2)}, u32[]{:S(2)}) %collective-permute-start.6) | collective-permute-done | bytes 327712 | tf_op jit(solution)/shard_map/ppermute | solution.py:268
  98.4 0.0 collective-permute-start.23
  98.5 2.9 %shard_map.57.rest_0_ = f32[1024,1280]{1,0:T(8,128)S(1)} custom-call(bf16[1024,2048]{1,0:T(8,128)(2,1)S(1)} %shard_map.55.x, bf16[10,128,128]{2,1,0:T(8,128)(2,1)S(1)} %collective-permute-done.2.rest_0_.rest_11_, bf16[10,128,128]{2,1,0:T(8,128)(2,1)S(1)} %collective-permute-done.6.rest_1_.rest_12_, ...), custom_call_target="tpu_custom_call" | custom-call | flops 2348810240 | bytes 10485760 | tf_op jit(solution)/shard_map/pallas_call | solution.py:145
  101.3 4.1 %collective-permute-done.17.rest_6_.rest_10_ = bf16[10,128,128]{2,1,0:T(8,128)(2,1)S(1)} collective-permute-done((bf16[10,128,128]{2,1,0:T(8,128)(2,1)S(1)}, bf16[10,128,128]{2,1,0:T(8,128)(2,1)S(1)}, u32[]{:S(2)}, u32[]{:S(2)}) %collective-permute-start.17) | collective-permute-done | bytes 327712 | tf_op jit(solution)/shard_map/ppermute | solution.py:268
  105.5 0.0 collective-permute-start.22
  105.5 7.0 %collective-permute-done.16.rest_4_.rest_8_ = bf16[10,128,128]{2,1,0:T(8,128)(2,1)S(1)} collective-permute-done((bf16[10,128,128]{2,1,0:T(8,128)(2,1)S(1)}, bf16[10,128,128]{2,1,0:T(8,128)(2,1)S(1)}, u32[]{:S(2)}, u32[]{:S(2)}) %collective-permute-start.16) | collective-permute-done | bytes 327712 | tf_op jit(solution)/shard_map/ppermute | solution.py:268
  112.5 7.0 %collective-permute-done.15.rest_2_.rest_6_ = bf16[10,128,128]{2,1,0:T(8,128)(2,1)S(1)} collective-permute-done((bf16[10,128,128]{2,1,0:T(8,128)(2,1)S(1)}, bf16[10,128,128]{2,1,0:T(8,128)(2,1)S(1)}, u32[]{:S(2)}, u32[]{:S(2)}) %collective-permute-start.15) | collective-permute-done | bytes 327712 | tf_op jit(solution)/shard_map/ppermute | solution.py:268
  119.4 2.7 %shard_map.58.a = f32[1024,1280]{1,0:T(8,128)S(1)} custom-call(bf16[1024,2048]{1,0:T(8,128)(2,1)S(1)} %shard_map.55.x, f32[1024,1280]{1,0:T(8,128)S(1)} %shard_map.57.rest_0_, bf16[10,128,128]{2,1,0:T(8,128)(2,1)S(1)} %collective-permute-done.11.rest_1_.rest_5_, ...), custom_call_target="tpu_custom_call", output_to_operand_aliasing={{}: (1, {})} | custom-call | flops 2013265920 | bytes 10485760 | tf_op jit(solution)/shard_map/pallas_call | solution.py:145
  122.2 0.7 collective-permute-done.23.rest_4_
  122.9 1.8 %collective-permute-done.22.rest_2_ = bf16[5,128,128]{2,1,0:T(8,128)(2,1)S(1)} collective-permute-done((bf16[5,128,128]{2,1,0:T(8,128)(2,1)S(1)}, bf16[5,128,128]{2,1,0:T(8,128)(2,1)S(1)}, u32[]{:S(2)}, u32[]{:S(2)}) %collective-permute-start.22) | collective-permute-done | bytes 163872 | tf_op jit(solution)/shard_map/ppermute | solution.py:268
  124.7 1.9 %shard_map.63 = (bf16[128,2048]{1,0:T(8,128)(2,1)S(1)}, bf16[128,2048]{1,0:T(8,128)(2,1)S(1)}) custom-call(s32[4]{0:T(128)S(1)} %pad_add_fusion.m, bf16[1024,2048]{1,0:T(8,128)(2,1)S(1)} %shard_map.55.x, f32[1024,1280]{1,0:T(8,128)S(1)} %shard_map.58.a, bf16[5,128,128]{2,1,0:T(8,128)(2,1)S(1)} %collective-permute-done.19.rest_0_, ...), custom_call_target="tpu_custom_call" | custom-call | flops 922746880 | bytes 8388608 | tf_op jit(solution)/shard_map/pallas_call | solution.py:183
  126.6 0.4 collective-permute-start.28
  127.0 1.9 %shard_map.61 = (bf16[128,2048]{1,0:T(8,128)(2,1)S(1)}, bf16[128,2048]{1,0:T(8,128)(2,1)S(1)}) custom-call(s32[4]{0:T(128)S(1)} %pad_add_fusion.m, bf16[1024,2048]{1,0:T(8,128)(2,1)S(1)} %shard_map.55.x, f32[1024,1280]{1,0:T(8,128)S(1)} %shard_map.58.a, bf16[5,128,128]{2,1,0:T(8,128)(2,1)S(1)} %collective-permute-done.19.rest_0_, ...), custom_call_target="tpu_custom_call" | custom-call | flops 922746880 | bytes 8388608 | tf_op jit(solution)/shard_map/pallas_call | solution.py:183
  128.9 0.6 collective-permute-start.26
  129.5 1.9 %shard_map.60 = (bf16[128,2048]{1,0:T(8,128)(2,1)S(1)}, bf16[128,2048]{1,0:T(8,128)(2,1)S(1)}) custom-call(s32[4]{0:T(128)S(1)} %pad_add_fusion.m, bf16[1024,2048]{1,0:T(8,128)(2,1)S(1)} %shard_map.55.x, f32[1024,1280]{1,0:T(8,128)S(1)} %shard_map.58.a, bf16[5,128,128]{2,1,0:T(8,128)(2,1)S(1)} %collective-permute-done.19.rest_0_, ...), custom_call_target="tpu_custom_call" | custom-call | flops 922746880 | bytes 8388608 | tf_op jit(solution)/shard_map/pallas_call | solution.py:183
  131.4 0.2 collective-permute-start.25
  131.6 1.9 %shard_map.59 = (bf16[128,2048]{1,0:T(8,128)(2,1)S(1)}, bf16[128,2048]{1,0:T(8,128)(2,1)S(1)}) custom-call(s32[4]{0:T(128)S(1)} %pad_add_fusion.m, bf16[1024,2048]{1,0:T(8,128)(2,1)S(1)} %shard_map.55.x, f32[1024,1280]{1,0:T(8,128)S(1)} %shard_map.58.a, bf16[5,128,128]{2,1,0:T(8,128)(2,1)S(1)} %collective-permute-done.19.rest_0_, ...), custom_call_target="tpu_custom_call" | custom-call | flops 922746880 | bytes 8388608 | tf_op jit(solution)/shard_map/pallas_call | solution.py:183
  133.5 0.1 shard_map.64
  133.6 1.7 %collective-permute-start.29 = (bf16[64,2048]{1,0:T(8,128)(2,1)S(1)}, bf16[64,2048]{1,0:T(8,128)(2,1)S(1)}, u32[]{:S(2)}, u32[]{:S(2)}) collective-permute-start(bf16[64,2048]{1,0:T(8,128)(2,1)S(1)} %get-tuple-element.32), channel_id=1, source_target_pairs={{0,2},{1,3},{2,4},{3,5},{4,6},{5,7},{6,0},{7,1},{8,10},{9,11},{10,... | collective-permute-start | bytes 786440 | tf_op jit(solution)/shard_map/ppermute | solution.py:262
  135.4 1.7 %collective-permute-start.30 = (bf16[64,2048]{1,0:T(8,128)(2,1)S(1)}, bf16[64,2048]{1,0:T(8,128)(2,1)S(1)}, u32[]{:S(2)}, u32[]{:S(2)}) collective-permute-start(bf16[64,2048]{1,0:T(8,128)(2,1)S(1)} %get-tuple-element.33), channel_id=1, source_target_pairs={{0,6},{1,7},{2,0},{3,1},{4,2},{5,3},{6,4},{7,5},{8,14},{9,15},{10,... | collective-permute-start | bytes 786440 | tf_op jit(solution)/shard_map/ppermute | solution.py:262
  137.1 0.2 collective-permute-start.24
  137.2 0.1 shard_map.62
  137.4 0.3 collective-permute-start.27
  137.7 3.0 %collective-permute-start.32 = (bf16[64,2048]{1,0:T(8,128)(2,1)S(1)}, bf16[64,2048]{1,0:T(8,128)(2,1)S(1)}, u32[]{:S(2)}, u32[]{:S(2)}) collective-permute-start(bf16[64,2048]{1,0:T(8,128)(2,1)S(1)} %get-tuple-element.35), channel_id=1, source_target_pairs={{0,6},{1,7},{2,0},{3,1},{4,2},{5,3},{6,4},{7,5},{8,14},{9,15},{10,... | collective-permute-start | bytes 786440 | tf_op jit(solution)/shard_map/ppermute | solution.py:262
  140.7 3.4 %collective-permute-done.29.rest_0_ = bf16[64,2048]{1,0:T(8,128)(2,1)S(1)} collective-permute-done((bf16[64,2048]{1,0:T(8,128)(2,1)S(1)}, bf16[64,2048]{1,0:T(8,128)(2,1)S(1)}, u32[]{:S(2)}, u32[]{:S(2)}) %collective-permute-start.29) | collective-permute-done | bytes 262176 | tf_op jit(solution)/shard_map/ppermute | solution.py:262
  144.1 0.4 collective-permute-done.30.rest_1_
  144.6 0.2 shard_map.65
  144.8 1.7 %collective-permute-start.31 = (bf16[64,2048]{1,0:T(8,128)(2,1)S(1)}, bf16[64,2048]{1,0:T(8,128)(2,1)S(1)}, u32[]{:S(2)}, u32[]{:S(2)}) collective-permute-start(bf16[64,2048]{1,0:T(8,128)(2,1)S(1)} %get-tuple-element.34), channel_id=1, source_target_pairs={{0,2},{1,3},{2,4},{3,5},{4,6},{5,7},{6,0},{7,1},{8,10},{9,11},{10,... | collective-permute-start | bytes 786440 | tf_op jit(solution)/shard_map/ppermute | solution.py:262
  146.5 1.6 %collective-permute-start.33 = (bf16[64,2048]{1,0:T(8,128)(2,1)S(1)}, bf16[64,2048]{1,0:T(8,128)(2,1)S(1)}, u32[]{:S(2)}, u32[]{:S(2)}) collective-permute-start(bf16[64,2048]{1,0:T(8,128)(2,1)S(1)} %get-tuple-element.36), channel_id=1, source_target_pairs={{0,6},{1,7},{2,0},{3,1},{4,2},{5,3},{6,4},{7,5},{8,14},{9,15},{10,... | collective-permute-start | bytes 786440 | tf_op jit(solution)/shard_map/ppermute | solution.py:262
  148.1 1.6 %collective-permute-done.27.f1 = bf16[64,2048]{1,0:T(8,128)(2,1)S(1)} collective-permute-done((bf16[64,2048]{1,0:T(8,128)(2,1)S(1)}, bf16[64,2048]{1,0:T(8,128)(2,1)S(1)}, u32[]{:S(2)}, u32[]{:S(2)}) %collective-permute-start.27) | collective-permute-done | bytes 262176 | tf_op jit(solution)/shard_map/ppermute | solution.py:262
  149.8 0.4 collective-permute-done.32.f3
  150.2 4.9 %collective-permute-done.31.r1 = bf16[64,2048]{1,0:T(8,128)(2,1)S(1)} collective-permute-done((bf16[64,2048]{1,0:T(8,128)(2,1)S(1)}, bf16[64,2048]{1,0:T(8,128)(2,1)S(1)}, u32[]{:S(2)}, u32[]{:S(2)}) %collective-permute-start.31) | collective-permute-done | bytes 262176 | tf_op jit(solution)/shard_map/ppermute | solution.py:262
  155.1 1.6 %shard_map.66 = bf16[128,2048]{1,0:T(8,128)(2,1)} custom-call(s32[4]{0:T(128)S(1)} %pad_add_fusion.m, bf16[128,2048]{1,0:T(8,128)(2,1)S(1)} %get-tuple-element.23.k, bf16[128,2048]{1,0:T(8,128)(2,1)S(1)} %collective-permute-done.24.g, bf16[64,2048]{1,0:T(8,128)(2,1)S(1)} %collective-permute-done.27.f1, bf16[64,2048]{1,0:T(8,128)(2,1)S(1)} %collective-permute-done.31.r1, ...), custom_call_target="tpu_custom_call" | custom-call | tf_op jit(solution)/shard_map/pallas_call | solution.py:246
  (39 shorter events, 0.5 us)
Async XLA Ops:
  1.8 30.3 %collective-permute-start = (bf16[10,128,128]{2,1,0:T(8,128)(2,1)S(1)}, bf16[10,128,128]{2,1,0:T(8,128)(2,1)S(1)}, u32[]{:S(2)}, u32[]{:S(2)}) collective-permute-start(bf16[10,128,128]{2,1,0:T(8,128)(2,1)S(1)} %get-tuple-element.21.rest_6_.rest_17_), channel_id=1, source_target_pairs={{0,8},{8,16},{16,24},{24,32},{32,40},{40,48},{48,56},{56,64},{64,7... | collective-permute-start | bytes 983048 | tf_op jit(solution)/shard_map/ppermute | solution.py:259
  4.7 27.4 %collective-permute-start.3 = (bf16[10,128,128]{2,1,0:T(8,128)(2,1)S(1)}, bf16[10,128,128]{2,1,0:T(8,128)(2,1)S(1)}, u32[]{:S(2)}, u32[]{:S(2)}) collective-permute-start(bf16[10,128,128]{2,1,0:T(8,128)(2,1)S(1)} %get-tuple-element.21.rest_6_.rest_17_), channel_id=1, source_target_pairs={{0,120},{8,0},{16,8},{24,16},{32,24},{40,32},{48,40},{56,48},{64,5... | collective-permute-start | bytes 983048 | tf_op jit(solution)/shard_map/ppermute | solution.py:259
  32.0 10.2 %collective-permute-start.1 = (bf16[10,128,128]{2,1,0:T(8,128)(2,1)S(1)}, bf16[10,128,128]{2,1,0:T(8,128)(2,1)S(1)}, u32[]{:S(2)}, u32[]{:S(2)}) collective-permute-start(bf16[10,128,128]{2,1,0:T(8,128)(2,1)S(1)} %collective-permute-done.rest_4_.rest_15_), channel_id=1, source_target_pairs={{0,8},{8,16},{16,24},{24,32},{32,40},{40,48},{48,56},{56,64},{64,7... | collective-permute-start | bytes 983048 | tf_op jit(solution)/shard_map/ppermute | solution.py:259
  32.1 10.2 %collective-permute-start.4 = (bf16[10,128,128]{2,1,0:T(8,128)(2,1)S(1)}, bf16[10,128,128]{2,1,0:T(8,128)(2,1)S(1)}, u32[]{:S(2)}, u32[]{:S(2)}) collective-permute-start(bf16[10,128,128]{2,1,0:T(8,128)(2,1)S(1)} %collective-permute-done.3.rest_8_.rest_19_), channel_id=1, source_target_pairs={{0,120},{8,0},{16,8},{24,16},{32,24},{40,32},{48,40},{56,48},{64,5... | collective-permute-start | bytes 983048 | tf_op jit(solution)/shard_map/ppermute | solution.py:259
  42.2 9.3 %collective-permute-start.2 = (bf16[10,128,128]{2,1,0:T(8,128)(2,1)S(1)}, bf16[10,128,128]{2,1,0:T(8,128)(2,1)S(1)}, u32[]{:S(2)}, u32[]{:S(2)}) collective-permute-start(bf16[10,128,128]{2,1,0:T(8,128)(2,1)S(1)} %collective-permute-done.1.rest_2_.rest_13_), channel_id=1, source_target_pairs={{0,8},{8,16},{16,24},{24,32},{32,40},{40,48},{48,56},{56,64},{64,7... | collective-permute-start | bytes 983048 | tf_op jit(solution)/shard_map/ppermute | solution.py:259
  42.2 9.3 %collective-permute-start.5 = (bf16[10,128,128]{2,1,0:T(8,128)(2,1)S(1)}, bf16[10,128,128]{2,1,0:T(8,128)(2,1)S(1)}, u32[]{:S(2)}, u32[]{:S(2)}) collective-permute-start(bf16[10,128,128]{2,1,0:T(8,128)(2,1)S(1)} %collective-permute-done.4.rest_9_.rest_20_), channel_id=1, source_target_pairs={{0,120},{8,0},{16,8},{24,16},{32,24},{40,32},{48,40},{56,48},{64,5... | collective-permute-start | bytes 983048 | tf_op jit(solution)/shard_map/ppermute | solution.py:259
  51.5 8.4 %collective-permute-start.9 = (bf16[10,128,128]{2,1,0:T(8,128)(2,1)S(1)}, bf16[10,128,128]{2,1,0:T(8,128)(2,1)S(1)}, u32[]{:S(2)}, u32[]{:S(2)}) collective-permute-start(bf16[10,128,128]{2,1,0:T(8,128)(2,1)S(1)} %collective-permute-done.2.rest_0_.rest_11_), channel_id=1, source_target_pairs={{0,8},{8,16},{16,24},{24,32},{32,40},{40,48},{48,56},{56,64},{64,7... | collective-permute-start | bytes 983048 | tf_op jit(solution)/shard_map/ppermute | solution.py:259
  51.5 8.4 %collective-permute-start.12 = (bf16[10,128,128]{2,1,0:T(8,128)(2,1)S(1)}, bf16[10,128,128]{2,1,0:T(8,128)(2,1)S(1)}, u32[]{:S(2)}, u32[]{:S(2)}) collective-permute-start(bf16[10,128,128]{2,1,0:T(8,128)(2,1)S(1)} %collective-permute-done.5.rest_10_.rest_21_), channel_id=1, source_target_pairs={{0,120},{8,0},{16,8},{24,16},{32,24},{40,32},{48,40},{56,48},{64,5... | collective-permute-start | bytes 983048 | tf_op jit(solution)/shard_map/ppermute | solution.py:259
  59.9 10.4 %collective-permute-start.10 = (bf16[10,128,128]{2,1,0:T(8,128)(2,1)S(1)}, bf16[10,128,128]{2,1,0:T(8,128)(2,1)S(1)}, u32[]{:S(2)}, u32[]{:S(2)}) collective-permute-start(bf16[10,128,128]{2,1,0:T(8,128)(2,1)S(1)} %collective-permute-done.9.rest_5_.rest_9_), channel_id=1, source_target_pairs={{0,8},{8,16},{16,24},{24,32},{32,40},{40,48},{48,56},{56,64},{64,7... | collective-permute-start | bytes 983048 | tf_op jit(solution)/shard_map/ppermute | solution.py:259
  59.9 10.5 %collective-permute-start.13 = (bf16[10,128,128]{2,1,0:T(8,128)(2,1)S(1)}, bf16[10,128,128]{2,1,0:T(8,128)(2,1)S(1)}, u32[]{:S(2)}, u32[]{:S(2)}) collective-permute-start(bf16[10,128,128]{2,1,0:T(8,128)(2,1)S(1)} %collective-permute-done.12.rest_7_.rest_22_), channel_id=1, source_target_pairs={{0,120},{8,0},{16,8},{24,16},{32,24},{40,32},{48,40},{56,48},{64,5... | collective-permute-start | bytes 983048 | tf_op jit(solution)/shard_map/ppermute | solution.py:259
  70.3 13.1 %collective-permute-start.11 = (bf16[10,128,128]{2,1,0:T(8,128)(2,1)S(1)}, bf16[10,128,128]{2,1,0:T(8,128)(2,1)S(1)}, u32[]{:S(2)}, u32[]{:S(2)}) collective-permute-start(bf16[10,128,128]{2,1,0:T(8,128)(2,1)S(1)} %collective-permute-done.10.rest_3_.rest_7_), channel_id=1, source_target_pairs={{0,8},{8,16},{16,24},{24,32},{32,40},{40,48},{48,56},{56,64},{64,7... | collective-permute-start | bytes 983048 | tf_op jit(solution)/shard_map/ppermute | solution.py:259
  70.4 9.2 %collective-permute-start.14 = (bf16[10,128,128]{2,1,0:T(8,128)(2,1)S(1)}, bf16[10,128,128]{2,1,0:T(8,128)(2,1)S(1)}, u32[]{:S(2)}, u32[]{:S(2)}) collective-permute-start(bf16[10,128,128]{2,1,0:T(8,128)(2,1)S(1)} %collective-permute-done.13.rest_8_.rest_23_), channel_id=1, source_target_pairs={{0,120},{8,0},{16,8},{24,16},{32,24},{40,32},{48,40},{56,48},{64,5... | collective-permute-start | bytes 983048 | tf_op jit(solution)/shard_map/ppermute | solution.py:259
  73.7 21.9 %collective-permute-start.8 = (bf16[10,128,128]{2,1,0:T(8,128)(2,1)S(1)}, bf16[10,128,128]{2,1,0:T(8,128)(2,1)S(1)}, u32[]{:S(2)}, u32[]{:S(2)}) collective-permute-start(bf16[10,128,128]{2,1,0:T(8,128)(2,1)S(1)} %pad_maximum_fusion.2), channel_id=1, source_target_pairs={{0,128},{128,0},{1,129},{129,1},{2,130},{130,2},{3,131},{131,3},{4... | collective-permute-start | bytes 983048 | tf_op jit(solution)/shard_map/ppermute | solution.py:268
  73.9 21.9 %collective-permute-start.7 = (bf16[10,128,128]{2,1,0:T(8,128)(2,1)S(1)}, bf16[10,128,128]{2,1,0:T(8,128)(2,1)S(1)}, u32[]{:S(2)}, u32[]{:S(2)}) collective-permute-start(bf16[10,128,128]{2,1,0:T(8,128)(2,1)S(1)} %pad_maximum_fusion.1), channel_id=1, source_target_pairs={{0,128},{128,0},{1,129},{129,1},{2,130},{130,2},{3,131},{131,3},{4... | collective-permute-start | bytes 983048 | tf_op jit(solution)/shard_map/ppermute | solution.py:268
  76.1 22.3 %collective-permute-start.6 = (bf16[10,128,128]{2,1,0:T(8,128)(2,1)S(1)}, bf16[10,128,128]{2,1,0:T(8,128)(2,1)S(1)}, u32[]{:S(2)}, u32[]{:S(2)}) collective-permute-start(bf16[10,128,128]{2,1,0:T(8,128)(2,1)S(1)} %pad_maximum_fusion), channel_id=1, source_target_pairs={{0,128},{128,0},{1,129},{129,1},{2,130},{130,2},{3,131},{131,3},{4... | collective-permute-start | bytes 983048 | tf_op jit(solution)/shard_map/ppermute | solution.py:268
  79.7 13.8 %collective-permute-start.20 = (bf16[10,128,128]{2,1,0:T(8,128)(2,1)S(1)}, bf16[10,128,128]{2,1,0:T(8,128)(2,1)S(1)}, u32[]{:S(2)}, u32[]{:S(2)}) collective-permute-start(bf16[10,128,128]{2,1,0:T(8,128)(2,1)S(1)} %collective-permute-done.14.rest_9_.rest_24_), channel_id=1, source_target_pairs={{0,120},{8,0},{16,8},{24,16},{32,24},{40,32},{48,40},{56,48},{64,5... | collective-permute-start | bytes 983048 | tf_op jit(solution)/shard_map/ppermute | solution.py:259
  83.4 10.0 %collective-permute-start.18 = (bf16[10,128,128]{2,1,0:T(8,128)(2,1)S(1)}, bf16[10,128,128]{2,1,0:T(8,128)(2,1)S(1)}, u32[]{:S(2)}, u32[]{:S(2)}) collective-permute-start(bf16[10,128,128]{2,1,0:T(8,128)(2,1)S(1)} %collective-permute-done.11.rest_1_.rest_5_), channel_id=1, source_target_pairs={{0,8},{8,16},{16,24},{24,32},{32,40},{40,48},{48,56},{56,64},{64,7... | collective-permute-start | bytes 983048 | tf_op jit(solution)/shard_map/ppermute | solution.py:259
  93.4 12.1 %collective-permute-start.17 = (bf16[10,128,128]{2,1,0:T(8,128)(2,1)S(1)}, bf16[10,128,128]{2,1,0:T(8,128)(2,1)S(1)}, u32[]{:S(2)}, u32[]{:S(2)}) collective-permute-start(bf16[10,128,128]{2,1,0:T(8,128)(2,1)S(1)} %pad_maximum_fusion.5), channel_id=1, source_target_pairs={{0,128},{128,0},{1,129},{129,1},{2,130},{130,2},{3,131},{131,3},{4... | collective-permute-start | bytes 983048 | tf_op jit(solution)/shard_map/ppermute | solution.py:268
  93.4 19.0 %collective-permute-start.16 = (bf16[10,128,128]{2,1,0:T(8,128)(2,1)S(1)}, bf16[10,128,128]{2,1,0:T(8,128)(2,1)S(1)}, u32[]{:S(2)}, u32[]{:S(2)}) collective-permute-start(bf16[10,128,128]{2,1,0:T(8,128)(2,1)S(1)} %pad_maximum_fusion.4), channel_id=1, source_target_pairs={{0,128},{128,0},{1,129},{129,1},{2,130},{130,2},{3,131},{131,3},{4... | collective-permute-start | bytes 983048 | tf_op jit(solution)/shard_map/ppermute | solution.py:268
  95.6 23.8 %collective-permute-start.15 = (bf16[10,128,128]{2,1,0:T(8,128)(2,1)S(1)}, bf16[10,128,128]{2,1,0:T(8,128)(2,1)S(1)}, u32[]{:S(2)}, u32[]{:S(2)}) collective-permute-start(bf16[10,128,128]{2,1,0:T(8,128)(2,1)S(1)} %pad_maximum_fusion.3), channel_id=1, source_target_pairs={{0,128},{128,0},{1,129},{129,1},{2,130},{130,2},{3,131},{131,3},{4... | collective-permute-start | bytes 983048 | tf_op jit(solution)/shard_map/ppermute | solution.py:268
  95.8 9.6 %collective-permute-start.19 = (bf16[5,128,128]{2,1,0:T(8,128)(2,1)S(1)}, bf16[5,128,128]{2,1,0:T(8,128)(2,1)S(1)}, u32[]{:S(2)}, u32[]{:S(2)}) collective-permute-start(bf16[5,128,128]{2,1,0:T(8,128)(2,1)S(1)} %slice.73), channel_id=1, source_target_pairs={{0,8},{8,16},{16,24},{24,32},{32,40},{40,48},{48,56},{56,64},{64,7... | collective-permute-start | bytes 491528 | tf_op jit(solution)/shard_map/ppermute | solution.py:259
  98.4 24.5 %collective-permute-start.23 = (bf16[10,128,128]{2,1,0:T(8,128)(2,1)S(1)}, bf16[10,128,128]{2,1,0:T(8,128)(2,1)S(1)}, u32[]{:S(2)}, u32[]{:S(2)}) collective-permute-start(bf16[10,128,128]{2,1,0:T(8,128)(2,1)S(1)} %pad_maximum_fusion.6), channel_id=1, source_target_pairs={{0,128},{128,0},{1,129},{129,1},{2,130},{130,2},{3,131},{131,3},{4... | collective-permute-start | bytes 983048 | tf_op jit(solution)/shard_map/ppermute | solution.py:268
  105.5 16.7 %collective-permute-start.21 = (bf16[5,128,128]{2,1,0:T(8,128)(2,1)S(1)}, bf16[5,128,128]{2,1,0:T(8,128)(2,1)S(1)}, u32[]{:S(2)}, u32[]{:S(2)}) collective-permute-start(bf16[5,128,128]{2,1,0:T(8,128)(2,1)S(1)} %get-tuple-element.38), channel_id=1, source_target_pairs={{0,120},{8,0},{16,8},{24,16},{32,24},{40,32},{48,40},{56,48},{64,5... | collective-permute-start | bytes 491528 | tf_op jit(solution)/shard_map/ppermute | solution.py:259
  105.5 19.2 %collective-permute-start.22 = (bf16[5,128,128]{2,1,0:T(8,128)(2,1)S(1)}, bf16[5,128,128]{2,1,0:T(8,128)(2,1)S(1)}, u32[]{:S(2)}, u32[]{:S(2)}) collective-permute-start(bf16[5,128,128]{2,1,0:T(8,128)(2,1)S(1)} %collective-permute-done.19.rest_0_), channel_id=1, source_target_pairs={{0,128},{128,0},{1,129},{129,1},{2,130},{130,2},{3,131},{131,3},{4... | collective-permute-start | bytes 491528 | tf_op jit(solution)/shard_map/ppermute | solution.py:268
  126.6 6.9 %collective-permute-start.28 = (bf16[128,2048]{1,0:T(8,128)(2,1)S(1)}, bf16[128,2048]{1,0:T(8,128)(2,1)S(1)}, u32[]{:S(2)}, u32[]{:S(2)}) collective-permute-start(bf16[128,2048]{1,0:T(8,128)(2,1)S(1)} %get-tuple-element.31), channel_id=1, source_target_pairs={{0,1},{1,0},{2,3},{3,2},{4,5},{5,4},{6,7},{7,6},{8,9},{9,8},{10,11... | collective-permute-start | bytes 1572872 | tf_op jit(solution)/shard_map/ppermute | solution.py:265
  128.9 8.3 %collective-permute-start.26 = (bf16[128,2048]{1,0:T(8,128)(2,1)S(1)}, bf16[128,2048]{1,0:T(8,128)(2,1)S(1)}, u32[]{:S(2)}, u32[]{:S(2)}) collective-permute-start(bf16[128,2048]{1,0:T(8,128)(2,1)S(1)} %get-tuple-element.28), channel_id=1, source_target_pairs={{0,1},{1,0},{2,3},{3,2},{4,5},{5,4},{6,7},{7,6},{8,9},{9,8},{10,11... | collective-permute-start | bytes 1572872 | tf_op jit(solution)/shard_map/ppermute | solution.py:265
  131.4 5.8 %collective-permute-start.25 = (bf16[128,2048]{1,0:T(8,128)(2,1)S(1)}, bf16[128,2048]{1,0:T(8,128)(2,1)S(1)}, u32[]{:S(2)}, u32[]{:S(2)}) collective-permute-start(bf16[128,2048]{1,0:T(8,128)(2,1)S(1)} %get-tuple-element.26), channel_id=1, source_target_pairs={{0,1},{1,0},{2,3},{3,2},{4,5},{5,4},{6,7},{7,6},{8,9},{9,8},{10,11... | collective-permute-start | bytes 1572872 | tf_op jit(solution)/shard_map/ppermute | solution.py:265
  133.6 10.5 %collective-permute-start.29 = (bf16[64,2048]{1,0:T(8,128)(2,1)S(1)}, bf16[64,2048]{1,0:T(8,128)(2,1)S(1)}, u32[]{:S(2)}, u32[]{:S(2)}) collective-permute-start(bf16[64,2048]{1,0:T(8,128)(2,1)S(1)} %get-tuple-element.32), channel_id=1, source_target_pairs={{0,2},{1,3},{2,4},{3,5},{4,6},{5,7},{6,0},{7,1},{8,10},{9,11},{10,... | collective-permute-start | bytes 786440 | tf_op jit(solution)/shard_map/ppermute | solution.py:262
  135.4 9.2 %collective-permute-start.30 = (bf16[64,2048]{1,0:T(8,128)(2,1)S(1)}, bf16[64,2048]{1,0:T(8,128)(2,1)S(1)}, u32[]{:S(2)}, u32[]{:S(2)}) collective-permute-start(bf16[64,2048]{1,0:T(8,128)(2,1)S(1)} %get-tuple-element.33), channel_id=1, source_target_pairs={{0,6},{1,7},{2,0},{3,1},{4,2},{5,3},{6,4},{7,5},{8,14},{9,15},{10,... | collective-permute-start | bytes 786440 | tf_op jit(solution)/shard_map/ppermute | solution.py:262
  137.1 11.1 %collective-permute-start.24 = (bf16[128,2048]{1,0:T(8,128)(2,1)S(1)}, bf16[128,2048]{1,0:T(8,128)(2,1)S(1)}, u32[]{:S(2)}, u32[]{:S(2)}) collective-permute-start(bf16[128,2048]{1,0:T(8,128)(2,1)S(1)} %get-tuple-element.24), channel_id=1, source_target_pairs={{0,1},{1,0},{2,3},{3,2},{4,5},{5,4},{6,7},{7,6},{8,9},{9,8},{10,11... | collective-permute-start | bytes 1572872 | tf_op jit(solution)/shard_map/ppermute | solution.py:265
  137.4 12.4 %collective-permute-start.27 = (bf16[64,2048]{1,0:T(8,128)(2,1)S(1)}, bf16[64,2048]{1,0:T(8,128)(2,1)S(1)}, u32[]{:S(2)}, u32[]{:S(2)}) collective-permute-start(bf16[64,2048]{1,0:T(8,128)(2,1)S(1)} %get-tuple-element.29), channel_id=1, source_target_pairs={{0,2},{1,3},{2,4},{3,5},{4,6},{5,7},{6,0},{7,1},{8,10},{9,11},{10,... | collective-permute-start | bytes 786440 | tf_op jit(solution)/shard_map/ppermute | solution.py:262
  137.7 12.5 %collective-permute-start.32 = (bf16[64,2048]{1,0:T(8,128)(2,1)S(1)}, bf16[64,2048]{1,0:T(8,128)(2,1)S(1)}, u32[]{:S(2)}, u32[]{:S(2)}) collective-permute-start(bf16[64,2048]{1,0:T(8,128)(2,1)S(1)} %get-tuple-element.35), channel_id=1, source_target_pairs={{0,6},{1,7},{2,0},{3,1},{4,2},{5,3},{6,4},{7,5},{8,14},{9,15},{10,... | collective-permute-start | bytes 786440 | tf_op jit(solution)/shard_map/ppermute | solution.py:262
  144.8 10.3 %collective-permute-start.31 = (bf16[64,2048]{1,0:T(8,128)(2,1)S(1)}, bf16[64,2048]{1,0:T(8,128)(2,1)S(1)}, u32[]{:S(2)}, u32[]{:S(2)}) collective-permute-start(bf16[64,2048]{1,0:T(8,128)(2,1)S(1)} %get-tuple-element.34), channel_id=1, source_target_pairs={{0,2},{1,3},{2,4},{3,5},{4,6},{5,7},{6,0},{7,1},{8,10},{9,11},{10,... | collective-permute-start | bytes 786440 | tf_op jit(solution)/shard_map/ppermute | solution.py:262
  146.5 8.6 %collective-permute-start.33 = (bf16[64,2048]{1,0:T(8,128)(2,1)S(1)}, bf16[64,2048]{1,0:T(8,128)(2,1)S(1)}, u32[]{:S(2)}, u32[]{:S(2)}) collective-permute-start(bf16[64,2048]{1,0:T(8,128)(2,1)S(1)} %get-tuple-element.36), channel_id=1, source_target_pairs={{0,6},{1,7},{2,0},{3,1},{4,2},{5,3},{6,4},{7,5},{8,14},{9,15},{10,... | collective-permute-start | bytes 786440 | tf_op jit(solution)/shard_map/ppermute | solution.py:262

commit v2 on v1

v2 whole, which is shorter than its diff:
```python
import functools

import jax
import jax.numpy as jnp
from jax import lax
from jax.experimental import pallas as pl
from jax.experimental.pallas import tpu as pltpu
from jax.sharding import PartitionSpec as P


EPSILON = 1e-06
B = 128
F32 = jnp.float32
BF16 = jnp.bfloat16


def hbm(v):
    return pltpu.with_memory_space_constraint(v, pltpu.HBM)


def vmem(mb):
    return pltpu.CompilerParams(vmem_limit_bytes=mb * 1024 * 1024)


def on_chip(n):
    return [pl.BlockSpec(memory_space=pltpu.VMEM)] * n


SLOTS = 5
SHARED = (("g", 0), ("g", 1), ("u", 0), ("u", 1), ("d", 0))
ALONE = (("g", 2), ("u", 2), ("d", 1), ("d", 2), ("d", 3))
PAIRED = tuple((what, SLOTS - 1 - k) for what, k in SHARED)


def other(names):
    return tuple((what, k + SLOTS) for what, k in names)


def own_first(names):
    return names + other(names)


def other_first(names):
    return other(names) + names


def pack(meta, gate, up, down):
    names = SHARED + ALONE + PAIRED

    def body(m, g, u, d, out):
        def put(flip):
            for n, (what, k) in enumerate(names):
                c = slice((SLOTS - 1 - k if flip else k) * B, (SLOTS - k if flip else k + 1) * B)
                out[n] = d[c, :] if what == "d" else (g if what == "g" else u)[:, c]

        pl.when(m[3] == 0)(lambda: put(False))
        pl.when(m[3] != 0)(lambda: put(True))

    whole = lambda v: pl.BlockSpec(v.shape, lambda i, m: (0, 0))
    return pl.pallas_call(
        body,
        grid_spec=pltpu.PrefetchScalarGridSpec(
            num_scalar_prefetch=1, grid=(1,), in_specs=[whole(gate), whole(up), whole(down)], out_specs=on_chip(1)[0]
        ),
        out_shape=pltpu.VMEM((len(names), B, B), gate.dtype),
        compiler_params=vmem(4),
    )(meta, hbm(gate), hbm(up), hbm(down))


def place(m, i, ring):
    o = i - ring // 2
    return lax.rem(m[2] + jnp.where(m[1] == 0, o, -o) + 2 * ring, ring)


def normalize(tokens, gain, meta, ring):
    rows, width = tokens.shape
    chips = rows // (2 * B)

    def body(m, t, g, out):
        block = lambda b: t[:, b * B:(b + 1) * B].astype(F32)
        square = block(0) * block(0)
        for b in range(1, ring):
            square = square + block(b) * block(b)
        scale = lax.rsqrt(jnp.sum(square, axis=-1, keepdims=True) * (1.0 / width) + EPSILON)
        at = pl.ds(pl.multiple_of(pl.program_id(0) * B, B), B)
        for b in range(ring):
            d = b - m[2] + ring
            i = lax.rem(jnp.where(m[1] == 0, d, 2 * ring - d) + ring // 2, ring)
            y = block(b) * scale * g[:, b * B:(b + 1) * B].astype(F32)
            out[at, pl.ds(pl.multiple_of(i * B, B), B)] = y.astype(BF16)

    return pl.pallas_call(
        body,
        grid_spec=pltpu.PrefetchScalarGridSpec(
            num_scalar_prefetch=1,
            grid=(chips,),
            in_specs=[pl.BlockSpec((B, width), lambda i, m: (2 * lax.rem(m[0] + i, chips) + m[1], 0)), pl.BlockSpec((1, width), lambda i, m: (0, 0))],
            out_specs=on_chip(1)[0],
        ),
        out_shape=pltpu.VMEM((chips * B, width), BF16),
        compiler_params=vmem(8),
        cost_estimate=pl.CostEstimate(flops=rows * width * 8, bytes_accessed=rows * width * 2, transcendentals=0),
    )(meta, hbm(tokens), gain.reshape(1, width))


class Parts:
    def __init__(self, pieces, ids):
        self.args, self.where = [], {}
        for i in ids:
            for array, lo, names in pieces[i]:
                n = next((n for n, v in enumerate(self.args) if v is array), len(self.args))
                if n == len(self.args):
                    self.args.append(array)
                for j, name in enumerate(names):
                    self.where[i, name] = (n, lo + j)

    def block(self, refs, i, name):
        n, j = self.where[i, name]
        return refs[n][j]

    def gate_up(self, refs, ids, k):
        rows = [jnp.concatenate([self.block(refs, i, ("g", k)), self.block(refs, i, ("u", k))], axis=1) for i in ids]
        return jnp.concatenate(rows, axis=0)

    def down(self, refs, ids):
        cols = [jnp.concatenate([self.block(refs, i, ("d", k)) for k in range(2 * SLOTS)], axis=0) for i in ids]
        return jnp.concatenate(cols, axis=1)


def runs(ids):
    out = []
    for i in ids:
        if out and out[-1][1] == i:
            out[-1][1] = i + 1
        else:
            out.append([i, i + 1])
    return out


def take(ref, rows, ids):
    cols = [ref[rows, a * B:b * B] for a, b in runs(ids)]
    return cols[0] if len(cols) == 1 else jnp.concatenate(cols, axis=1)


def accumulate(normed, ids, pieces, acc):
    rows = normed.shape[0]
    gu = Parts(pieces, ids)
    old = [] if acc is None else [acc]

    def body(x, *rest):
        refs, out = rest[len(old):-1], rest[-1]
        v = take(x, slice(0, rows), ids)
        for k in range(2 * SLOTS):
            c = slice(2 * k * B, 2 * (k + 1) * B)
            part = jnp.dot(v, gu.gate_up(refs, ids, k), preferred_element_type=F32)
            out[:, c] = rest[0][:, c] + part if old else part

    return pl.pallas_call(
        body,
        in_specs=on_chip(1 + len(old) + len(gu.args)),
        out_specs=on_chip(1)[0],
        out_shape=pltpu.VMEM((rows, 4 * SLOTS * B), F32),
        input_output_aliases={1: 0} if old else {},
        compiler_params=vmem(6),
        cost_estimate=pl.CostEstimate(flops=8 * rows * len(ids) * B * SLOTS * B, bytes_accessed=rows * SLOTS * B * 32, transcendentals=0),
    )(normed, *old, *gu.args)


def finish(normed, ids, pieces, acc, rels, outs):
    ring = len(pieces)
    parts = Parts(pieces, range(ring))
    many = len(rels) * B

    def body(x, a, *rest):
        refs, out = rest[:len(parts.args)], rest[len(parts.args):]
        row = [slice(r * B, (r + 1) * B) for r in rels]
        v = jnp.concatenate([take(x, r, ids) for r in row], axis=0)
        h = []
        for k in range(2 * SLOTS):
            c = slice(2 * k * B, 2 * (k + 1) * B)
            act = jnp.concatenate([a[r, c] for r in row], axis=0)
            act = act + jnp.dot(v, parts.gate_up(refs, ids, k), preferred_element_type=F32)
            gate = act[:, :B]
            h.append((gate / (1.0 + jnp.exp(-gate)) * act[:, B:]).astype(BF16))
        h = jnp.concatenate(h, axis=1)
        for j in range(0, ring, 2):
            c = slice(j * B, (j + 2) * B)
            y = jnp.dot(h, parts.down(refs, [j, j + 1]), preferred_element_type=F32)
            for o, (rel, rows, kind) in zip(out, outs):
                lo = rels.index(rel) * B
                o[:, c] = y[lo + rows.start:lo + rows.stop].astype(kind)

    return pl.pallas_call(
        body,
        in_specs=on_chip(2 + len(parts.args)),
        out_specs=on_chip(len(outs)),
        out_shape=[pltpu.VMEM((rows.stop - rows.start, ring * B), kind) for _, rows, kind in outs],
        compiler_params=vmem(6),
        cost_estimate=pl.CostEstimate(flops=4 * many * SLOTS * B * (2 * len(ids) * B + ring * B), bytes_accessed=8 << 20, transcendentals=many * 2 * SLOTS * B),
    )(normed, acc, *parts.args)


def add(pairs):
    def body(*refs):
        n = len(pairs)
        for i in range(n):
            refs[2 * n + i][...] = (refs[2 * i][...] + refs[2 * i + 1][...].astype(F32)).astype(BF16)

    return pl.pallas_call(
        body, in_specs=on_chip(2 * len(pairs)), out_specs=on_chip(len(pairs)),
        out_shape=[pltpu.VMEM(p.shape, BF16) for p, _ in pairs], compiler_params=vmem(4),
    )(*[v for p in pairs for v in p])


def total(meta, keep, free1, rest1, free3, rest3, ring):
    rows, cols = keep.shape
    h = rows // 2

    def body(m, k, f1, r1, f3, r3, out):
        for j in range(ring):
            c = slice(j * B, (j + 1) * B)
            at = pl.ds(pl.multiple_of(place(m, j, ring) * B, B), B)
            out[:h, at] = (k[:h, c] + (r1[:, c].astype(F32) + f3[:, c].astype(F32))).astype(BF16)
            out[h:, at] = (k[h:, c] + (f1[:, c].astype(F32) + r3[:, c].astype(F32))).astype(BF16)

    return pl.pallas_call(
        body,
        in_specs=[pl.BlockSpec(memory_space=pltpu.SMEM)] + on_chip(5),
        out_specs=pl.BlockSpec((rows, cols), lambda: (0, 0)),
        out_shape=jax.ShapeDtypeStruct((rows, cols), BF16),
        compiler_params=vmem(4),
    )(meta, keep, free1, rest1, free3, rest3)


def on_device(sizes, tokens, norm_gain, gate_weight, up_weight, down_weight):
    ring, tp, groups = sizes["fs"], sizes["tp"], sizes["grp"]
    half = ring // 2

    def shift(v):
        way = [(i * tp + t, (i + 1 - 2 * (t % 2)) % ring * tp + t) for i in range(ring) for t in range(tp)]
        return lax.ppermute(v, ("fs", "tp"), way)

    def chip(v, k):
        return lax.ppermute(v, "tp", [(i, (i + 2 * k) % tp) for i in range(tp)])

    def core(v):
        return lax.ppermute(v, "tp", [(i, i ^ 1) for i in range(tp)])

    def pair(v):
        return lax.ppermute(v, "grp", [(i, i ^ 1) for i in range(groups)])

    def join(*parts):
        return jnp.concatenate(parts)

    t = lax.axis_index("tp")
    meta = jnp.stack([t // 2, t % 2, lax.axis_index("fs"), lax.axis_index("grp") % 2]).astype(jnp.int32)
    n = len(SHARED)

    own = pack(meta, gate_weight, up_weight, down_weight)
    theirs = core(own)
    every = SHARED + ALONE + PAIRED
    pieces = {half: [(own, 0, every), (theirs, 0, other(every))]}
    m = join(own[:n], theirs[:n])
    a = join(own[n:2 * n], theirs[n:2 * n])
    waiting = []

    def forward():
        d, at = core(join(*[v for v, _, _ in waiting])), 0
        for v, i, names in waiting:
            pieces[i].append((d, at, names))
            at += len(names)
        waiting.clear()

    for s in range(1, half):
        m = shift(m)
        a = shift(a)
        pieces[half - s] = [(m, 0, own_first(SHARED)), (a, 0, own_first(ALONE))]
        pieces[half + s] = []
        waiting += [(m, half + s, other_first(SHARED)), (a, half + s, other_first(ALONE))]
        if s > 1:
            forward()
        y = pair(m)
        pieces[half - s].append((y, 0, own_first(PAIRED)))
        waiting.append((y, half + s, other_first(PAIRED)))
    m = jnp.concatenate([m[:n], a[:n]])
    m = shift(m)
    pieces[0] = [(m, 0, SHARED + ALONE)]
    waiting.append((m, 0, other(SHARED + ALONE)))
    forward()
    y = pair(m[:n])
    pieces[0] += [(y, 0, PAIRED), (core(y), 0, other(PAIRED))]
    normed = normalize(tokens, norm_gain, meta, ring)
    acc = accumulate(normed, list(range(half - 3, half + 4)), pieces, None)
    acc = accumulate(normed, [2, 3, 4, ring - 4, ring - 3, ring - 2], pieces, acc)
    last = [0, 1, ring - 1]
    top, low = slice(0, B // 2), slice(B // 2, B)
    a, b = finish(normed, last, pieces, acc, [2], [(2, top, BF16), (2, low, BF16)])
    a, b = chip(a, 1), chip(b, -1)
    f1, w1, f3, w3 = finish(normed, last, pieces, acc, [1, 3], [(1, low, BF16), (1, top, F32), (3, top, BF16), (3, low, F32)])
    f1, f3 = chip(f1, 1), chip(f3, -1)
    (keep,) = finish(normed, last, pieces, acc, [0], [(0, slice(0, B), F32)])
    r1, r3 = add(((w1, a), (w3, b)))
    r1, r3 = chip(r1, 1), chip(r3, -1)
    return total(meta, keep, f1, r1, f3, r3, ring)


def solution(mesh):
    spec = P(("grp", "fs"), None)
    return jax.shard_map(
        functools.partial(on_device, dict(mesh.shape)),
        mesh=mesh,
        in_specs=(spec, P(), P("fs", "tp"), P("fs", "tp"), P("tp", "fs")),
        out_specs=P(("grp", "fs", "tp"), None),
        check_vma=False,
    )
```

time: 158 us -> 151 us (0.956)
  starting transfers between devices: 58.9 us -> 23.3 us
  waiting for transfers between devices: 72.9 us -> 108 us
  Pallas kernels: 23.4 us -> 17 us
    ppermute x16 -> x15, starting transfers between devices: 42.7 us -> 5.81 us  [shift(): return lax.ppermute(v, ('fs', 'tp'), way)]
    ppermute x16 -> x15, waiting for transfers between devices: 39.1 us -> 62.2 us  [shift(): return lax.ppermute(v, ('fs', 'tp'), way)]
    ppermute x8, waiting for transfers between devices: 23.1 us -> 35.9 us  [pair(): return lax.ppermute(v, 'grp', [(i, i ^ 1) for i in range(groups)])]
    pallas_call x8 -> x5, Pallas kernels: 9.71 us -> 6.33 us  [the longest x3 4.71 us: finish(): pl.pallas_call(body, in_specs=on_chip(2 + len(parts.args)), out_specs=on_...]
    ppermute x6, waiting for transfers between devices: 10.8 us -> 7.83 us  [chip(): return lax.ppermute(v, 'tp', [(i, (i + 2 * k) % tp) for i in range(tp)])]
    pallas_call x1, Pallas kernels: 6.37 us -> 3.69 us  [normalize(): pl.pallas_call(body, grid_spec=pltpu.PrefetchScalarGridSpec(num_scalar_pr...]
    ppermute x4 -> x9, waiting for transfers between devices: 0.01 us -> 1.83 us  [core(): return lax.ppermute(v, 'tp', [(i, i ^ 1) for i in range(tp)])]
  transfers between devices with their start and end apart: 34 -> 38, of which waited for: 17 -> 26; matrix products, arithmetic and copies ran while one was open for 1% -> 1% of each run, Pallas kernels for 12% -> 8%
where the time goes in v2:
time: 151 us; the launch traced here: 149 us
  waiting for transfers between devices  108 us (72%)
  starting transfers between devices  23.3 us (15%)
  Pallas kernels  17 us (11%)
    ppermute x15, waiting for transfers between devices, shift(): return lax.ppermute(v, ('fs', 'tp'), way)  62.2 us
    ppermute x8, waiting for transfers between devices, pair(): return lax.ppermute(v, 'grp', [(i, i ^ 1) for i in range(groups)])  35.9 us
    ppermute x6, starting transfers between devices, chip(): return lax.ppermute(v, 'tp', [(i, (i + 2 * k) % tp) for i in range(tp)])  10.1 us
    ppermute x6, waiting for transfers between devices, chip(): return lax.ppermute(v, 'tp', [(i, (i + 2 * k) % tp) for i in range(tp)])  7.83 us
    ppermute x15, starting transfers between devices, shift(): return lax.ppermute(v, ('fs', 'tp'), way)  5.81 us
    ppermute x8, starting transfers between devices, pair(): return lax.ppermute(v, 'grp', [(i, i ^ 1) for i in range(groups)])  5.39 us
    pallas_call x2, Pallas kernels, accumulate(): pl.pallas_call(body, in_specs=on_chip(1 + len(old) + len(gu.args)), out_s...  5.33 us
    pallas_call x3, Pallas kernels, finish(): pl.pallas_call(body, in_specs=on_chip(2 + len(parts.args)), out_specs=on_...  4.71 us
  transfers between devices with their start and end apart: 38, of which 26 were waited for; matrix products, arithmetic and copies ran while one was open for 1% of the time, Pallas kernels for 8%

profile of v2, /device:TPU:40, one launch (start us, length us, event | category | flops | bytes accessed | tf_op | source)
XLA Modules:
  0.0 149.5 jit_solution(17179679899490690510)
XLA Ops:
  0.0 0.1 pad_add_fusion.m
  0.1 1.7 %shard_map.56.rest_9_.rest_25_ = bf16[15,128,128]{2,1,0:T(8,128)(2,1)S(1)} custom-call(s32[4]{0:T(128)S(1)} %pad_add_fusion.m, bf16[128,640]{1,0:T(8,128)(2,1)} %g.1, bf16[128,640]{1,0:T(8,128)(2,1)} %u.1, bf16[640,128]{1,0:T(8,128)(2,1)} %d.1), custom_call_target="tpu_custom_call" | custom-call | tf_op jit(solution)/shard_map/pallas_call | solution.py:60
  1.8 0.1 collective-permute-start
  1.9 1.8 %collective-permute-done.rest_10_.rest_26_ = bf16[15,128,128]{2,1,0:T(8,128)(2,1)S(1)} collective-permute-done((bf16[15,128,128]{2,1,0:T(8,128)(2,1)S(1)}, bf16[15,128,128]{2,1,0:T(8,128)(2,1)S(1)}, u32[]{:S(2)}, u32[]{:S(2)}) %collective-permute-start) | collective-permute-done | bytes 491552 | tf_op jit(solution)/shard_map/ppermute | solution.py:247
  3.8 2.9 %collective-permute-start.1 = (bf16[10,128,128]{2,1,0:T(8,128)(2,1)S(1)}, bf16[10,128,128]{2,1,0:T(8,128)(2,1)S(1)}, u32[]{:S(2)}, u32[]{:S(2)}) collective-permute-start(bf16[10,128,128]{2,1,0:T(8,128)(2,1)S(1)} %pad_maximum_fusion.6), channel_id=1, source_target_pairs={{0,8},{1,121},{2,10},{3,123},{4,12},{5,125},{6,14},{7,127},{8,16},... | collective-permute-start | bytes 983048 | tf_op jit(solution)/shard_map/ppermute | solution.py:241
  6.7 2.9 %collective-permute-start.4 = (bf16[10,128,128]{2,1,0:T(8,128)(2,1)S(1)}, bf16[10,128,128]{2,1,0:T(8,128)(2,1)S(1)}, u32[]{:S(2)}, u32[]{:S(2)}) collective-permute-start(bf16[10,128,128]{2,1,0:T(8,128)(2,1)S(1)} %pad_maximum_fusion.7), channel_id=1, source_target_pairs={{0,8},{1,121},{2,10},{3,123},{4,12},{5,125},{6,14},{7,127},{8,16},... | collective-permute-start | bytes 983048 | tf_op jit(solution)/shard_map/ppermute | solution.py:241
  9.6 21.7 %collective-permute-done.1.rest_6_.rest_22_ = bf16[10,128,128]{2,1,0:T(8,128)(2,1)S(1)} collective-permute-done((bf16[10,128,128]{2,1,0:T(8,128)(2,1)S(1)}, bf16[10,128,128]{2,1,0:T(8,128)(2,1)S(1)}, u32[]{:S(2)}, u32[]{:S(2)}) %collective-permute-start.1) | collective-permute-done | bytes 327712 | tf_op jit(solution)/shard_map/ppermute | solution.py:241
  31.4 3.5 %collective-permute-done.4.rest_7_.rest_23_ = bf16[10,128,128]{2,1,0:T(8,128)(2,1)S(1)} collective-permute-done((bf16[10,128,128]{2,1,0:T(8,128)(2,1)S(1)}, bf16[10,128,128]{2,1,0:T(8,128)(2,1)S(1)}, u32[]{:S(2)}, u32[]{:S(2)}) %collective-permute-start.4) | collective-permute-done | bytes 327712 | tf_op jit(solution)/shard_map/ppermute | solution.py:241
  34.9 4.8 %collective-permute-done.2.rest_3_.rest_19_ = bf16[10,128,128]{2,1,0:T(8,128)(2,1)S(1)} collective-permute-done((bf16[10,128,128]{2,1,0:T(8,128)(2,1)S(1)}, bf16[10,128,128]{2,1,0:T(8,128)(2,1)S(1)}, u32[]{:S(2)}, u32[]{:S(2)}) %collective-permute-start.2) | collective-permute-done | bytes 327712 | tf_op jit(solution)/shard_map/ppermute | solution.py:241
  39.7 3.5 %collective-permute-done.5.rest_4_.rest_20_ = bf16[10,128,128]{2,1,0:T(8,128)(2,1)S(1)} collective-permute-done((bf16[10,128,128]{2,1,0:T(8,128)(2,1)S(1)}, bf16[10,128,128]{2,1,0:T(8,128)(2,1)S(1)}, u32[]{:S(2)}, u32[]{:S(2)}) %collective-permute-start.5) | collective-permute-done | bytes 327712 | tf_op jit(solution)/shard_map/ppermute | solution.py:241
  43.2 4.8 %collective-permute-done.3.rest_0_.rest_16_ = bf16[10,128,128]{2,1,0:T(8,128)(2,1)S(1)} collective-permute-done((bf16[10,128,128]{2,1,0:T(8,128)(2,1)S(1)}, bf16[10,128,128]{2,1,0:T(8,128)(2,1)S(1)}, u32[]{:S(2)}, u32[]{:S(2)}) %collective-permute-start.3) | collective-permute-done | bytes 327712 | tf_op jit(solution)/shard_map/ppermute | solution.py:241
  47.9 3.5 %collective-permute-done.6.rest_1_.rest_17_ = bf16[10,128,128]{2,1,0:T(8,128)(2,1)S(1)} collective-permute-done((bf16[10,128,128]{2,1,0:T(8,128)(2,1)S(1)}, bf16[10,128,128]{2,1,0:T(8,128)(2,1)S(1)}, u32[]{:S(2)}, u32[]{:S(2)}) %collective-permute-start.6) | collective-permute-done | bytes 327712 | tf_op jit(solution)/shard_map/ppermute | solution.py:241
  51.5 4.8 %collective-permute-done.12.rest_7_.rest_13_ = bf16[10,128,128]{2,1,0:T(8,128)(2,1)S(1)} collective-permute-done((bf16[10,128,128]{2,1,0:T(8,128)(2,1)S(1)}, bf16[10,128,128]{2,1,0:T(8,128)(2,1)S(1)}, u32[]{:S(2)}, u32[]{:S(2)}) %collective-permute-start.12) | collective-permute-done | bytes 327712 | tf_op jit(solution)/shard_map/ppermute | solution.py:241
  56.2 3.5 %collective-permute-done.13.rest_8_.rest_14_ = bf16[10,128,128]{2,1,0:T(8,128)(2,1)S(1)} collective-permute-done((bf16[10,128,128]{2,1,0:T(8,128)(2,1)S(1)}, bf16[10,128,128]{2,1,0:T(8,128)(2,1)S(1)}, u32[]{:S(2)}, u32[]{:S(2)}) %collective-permute-start.13) | collective-permute-done | bytes 327712 | tf_op jit(solution)/shard_map/ppermute | solution.py:241
  59.8 2.1 %collective-permute-start.8 = (bf16[10,128,128]{2,1,0:T(8,128)(2,1)S(1)}, bf16[10,128,128]{2,1,0:T(8,128)(2,1)S(1)}, u32[]{:S(2)}, u32[]{:S(2)}) collective-permute-start(bf16[10,128,128]{2,1,0:T(8,128)(2,1)S(1)} %collective-permute-done.2.rest_3_.rest_19_), channel_id=1, source_target_pairs={{0,128},{128,0},{1,129},{129,1},{2,130},{130,2},{3,131},{131,3},{4... | collective-permute-start | bytes 983048 | tf_op jit(solution)/shard_map/ppermute | solution.py:250
  62.0 2.5 %collective-permute-done.15.rest_4_.rest_10_ = bf16[10,128,128]{2,1,0:T(8,128)(2,1)S(1)} collective-permute-done((bf16[10,128,128]{2,1,0:T(8,128)(2,1)S(1)}, bf16[10,128,128]{2,1,0:T(8,128)(2,1)S(1)}, u32[]{:S(2)}, u32[]{:S(2)}) %collective-permute-start.15) | collective-permute-done | bytes 327712 | tf_op jit(solution)/shard_map/ppermute | solution.py:241
  64.5 3.5 %collective-permute-done.17.rest_5_.rest_11_ = bf16[10,128,128]{2,1,0:T(8,128)(2,1)S(1)} collective-permute-done((bf16[10,128,128]{2,1,0:T(8,128)(2,1)S(1)}, bf16[10,128,128]{2,1,0:T(8,128)(2,1)S(1)}, u32[]{:S(2)}, u32[]{:S(2)}) %collective-permute-start.17) | collective-permute-done | bytes 327712 | tf_op jit(solution)/shard_map/ppermute | solution.py:241
  68.0 2.3 %collective-permute-done.9.rest_8_.rest_24_ = bf16[10,128,128]{2,1,0:T(8,128)(2,1)S(1)} collective-permute-done((bf16[10,128,128]{2,1,0:T(8,128)(2,1)S(1)}, bf16[10,128,128]{2,1,0:T(8,128)(2,1)S(1)}, u32[]{:S(2)}, u32[]{:S(2)}) %collective-permute-start.9) | collective-permute-done | bytes 327712 | tf_op jit(solution)/shard_map/ppermute | solution.py:250
  70.5 0.3 collective-permute-start.10
  70.8 0.1 collective-permute-start.7
  71.0 1.8 %collective-permute-done.16.rest_1_.rest_7_ = bf16[10,128,128]{2,1,0:T(8,128)(2,1)S(1)} collective-permute-done((bf16[10,128,128]{2,1,0:T(8,128)(2,1)S(1)}, bf16[10,128,128]{2,1,0:T(8,128)(2,1)S(1)}, u32[]{:S(2)}, u32[]{:S(2)}) %collective-permute-start.16) | collective-permute-done | bytes 327712 | tf_op jit(solution)/shard_map/ppermute | solution.py:241
  72.8 3.5 %collective-permute-done.18.rest_2_.rest_8_ = bf16[10,128,128]{2,1,0:T(8,128)(2,1)S(1)} collective-permute-done((bf16[10,128,128]{2,1,0:T(8,128)(2,1)S(1)}, bf16[10,128,128]{2,1,0:T(8,128)(2,1)S(1)}, u32[]{:S(2)}, u32[]{:S(2)}) %collective-permute-start.18) | collective-permute-done | bytes 327712 | tf_op jit(solution)/shard_map/ppermute | solution.py:241
  76.3 0.1 pad_maximum_fusion
  76.4 0.1 collective-permute-start.11
  76.6 5.3 %collective-permute-done.7.rest_2_.rest_18_ = bf16[10,128,128]{2,1,0:T(8,128)(2,1)S(1)} collective-permute-done((bf16[10,128,128]{2,1,0:T(8,128)(2,1)S(1)}, bf16[10,128,128]{2,1,0:T(8,128)(2,1)S(1)}, u32[]{:S(2)}, u32[]{:S(2)}) %collective-permute-start.7) | collective-permute-done | bytes 327712 | tf_op jit(solution)/shard_map/ppermute | solution.py:250
  81.9 0.3 collective-permute-start.21
  82.2 1.7 %collective-permute-start.20 = (bf16[10,128,128]{2,1,0:T(8,128)(2,1)S(1)}, bf16[10,128,128]{2,1,0:T(8,128)(2,1)S(1)}, u32[]{:S(2)}, u32[]{:S(2)}) collective-permute-start(bf16[10,128,128]{2,1,0:T(8,128)(2,1)S(1)} %collective-permute-done.15.rest_4_.rest_10_), channel_id=1, source_target_pairs={{0,128},{128,0},{1,129},{129,1},{2,130},{130,2},{3,131},{131,3},{4... | collective-permute-start | bytes 983048 | tf_op jit(solution)/shard_map/ppermute | solution.py:250
  83.9 0.7 collective-permute-done.25.rest_5_
  84.6 0.2 collective-permute-start.19
  84.8 0.1 pad_maximum_fusion.1
  85.0 7.5 %collective-permute-done.21.rest_9_.rest_15_ = bf16[10,128,128]{2,1,0:T(8,128)(2,1)S(1)} collective-permute-done((bf16[10,128,128]{2,1,0:T(8,128)(2,1)S(1)}, bf16[10,128,128]{2,1,0:T(8,128)(2,1)S(1)}, u32[]{:S(2)}, u32[]{:S(2)}) %collective-permute-start.21) | collective-permute-done | bytes 327712 | tf_op jit(solution)/shard_map/ppermute | solution.py:250
  92.5 7.0 %collective-permute-done.20.rest_6_.rest_12_ = bf16[10,128,128]{2,1,0:T(8,128)(2,1)S(1)} collective-permute-done((bf16[10,128,128]{2,1,0:T(8,128)(2,1)S(1)}, bf16[10,128,128]{2,1,0:T(8,128)(2,1)S(1)}, u32[]{:S(2)}, u32[]{:S(2)}) %collective-permute-start.20) | collective-permute-done | bytes 327712 | tf_op jit(solution)/shard_map/ppermute | solution.py:250
  99.5 0.3 collective-permute-start.28
  99.8 0.1 pad_maximum_fusion.2
  99.9 6.6 %collective-permute-done.19.rest_3_.rest_9_ = bf16[10,128,128]{2,1,0:T(8,128)(2,1)S(1)} collective-permute-done((bf16[10,128,128]{2,1,0:T(8,128)(2,1)S(1)}, bf16[10,128,128]{2,1,0:T(8,128)(2,1)S(1)}, u32[]{:S(2)}, u32[]{:S(2)}) %collective-permute-start.19) | collective-permute-done | bytes 327712 | tf_op jit(solution)/shard_map/ppermute | solution.py:250
  106.5 0.1 pad_maximum_fusion.3
  106.6 0.0 copy-start
  106.6 0.1 pad_maximum_fusion.4
  106.8 0.6 collective-permute-start.22
  107.4 0.2 collective-permute-start.23
  107.5 4.2 %collective-permute-done.28.rest_6_ = bf16[10,128,128]{2,1,0:T(8,128)(2,1)S(1)} collective-permute-done((bf16[10,128,128]{2,1,0:T(8,128)(2,1)S(1)}, bf16[10,128,128]{2,1,0:T(8,128)(2,1)S(1)}, u32[]{:S(2)}, u32[]{:S(2)}) %collective-permute-start.28) | collective-permute-done | bytes 327712 | tf_op jit(solution)/shard_map/ppermute | solution.py:250
  111.7 0.1 pad_maximum_fusion.5
  111.8 0.6 collective-permute-start.29
  112.4 3.7 %shard_map.55.x = bf16[512,2048]{1,0:T(8,128)(2,1)S(1)} custom-call(s32[4]{0:T(128)S(1)} %pad_add_fusion.m, bf16[1024,2048]{1,0:T(8,128)(2,1)} %t.1, bf16[1,2048]{1,0:T(2,128)(2,1)S(1)} %reshape.3.g), custom_call_target="tpu_custom_call" | custom-call | flops 16777216 | bytes 4194304 | tf_op jit(solution)/shard_map/pallas_call | solution.py:92
  116.2 0.6 collective-permute-start.30
  116.8 2.9 %shard_map.57.rest_0_ = f32[512,2560]{1,0:T(8,128)S(1)} custom-call(bf16[512,2048]{1,0:T(8,128)(2,1)S(1)} %shard_map.55.x, bf16[10,128,128]{2,1,0:T(8,128)(2,1)S(1)} %collective-permute-done.3.rest_0_.rest_16_, bf16[10,128,128]{2,1,0:T(8,128)(2,1)S(1)} %collective-permute-done.6.rest_1_.rest_17_, ...), custom_call_target="tpu_custom_call" | custom-call | flops 2348810240 | bytes 10485760 | tf_op jit(solution)/shard_map/pallas_call | solution.py:158
  119.7 3.0 %collective-permute-done.30.rest_2_ = bf16[5,128,128]{2,1,0:T(8,128)(2,1)S(1)} collective-permute-done((bf16[5,128,128]{2,1,0:T(8,128)(2,1)S(1)}, bf16[5,128,128]{2,1,0:T(8,128)(2,1)S(1)}, u32[]{:S(2)}, u32[]{:S(2)}) %collective-permute-start.30) | collective-permute-done | bytes 163872 | tf_op jit(solution)/shard_map/ppermute | solution.py:250
  122.7 2.5 %shard_map.58.a = f32[512,2560]{1,0:T(8,128)S(1)} custom-call(bf16[512,2048]{1,0:T(8,128)(2,1)S(1)} %shard_map.55.x, f32[512,2560]{1,0:T(8,128)S(1)} %shard_map.57.rest_0_, bf16[10,128,128]{2,1,0:T(8,128)(2,1)S(1)} %collective-permute-done.16.rest_1_.rest_7_, ...), custom_call_target="tpu_custom_call", output_to_operand_aliasing={{}: (1, {})} | custom-call | flops 2013265920 | bytes 10485760 | tf_op jit(solution)/shard_map/pallas_call | solution.py:158
  125.2 1.3 shard_map.61
  126.4 1.7 %collective-permute-start.33 = (bf16[64,2048]{1,0:T(8,128)(2,1)S(1)}, bf16[64,2048]{1,0:T(8,128)(2,1)S(1)}, u32[]{:S(2)}, u32[]{:S(2)}) collective-permute-start(bf16[64,2048]{1,0:T(8,128)(2,1)S(1)} %get-tuple-element.15), channel_id=1, source_target_pairs={{0,2},{1,3},{2,4},{3,5},{4,6},{5,7},{6,0},{7,1},{8,10},{9,11},{10,... | collective-permute-start | bytes 786440 | tf_op jit(solution)/shard_map/ppermute | solution.py:244
  128.2 1.7 %collective-permute-start.34 = (bf16[64,2048]{1,0:T(8,128)(2,1)S(1)}, bf16[64,2048]{1,0:T(8,128)(2,1)S(1)}, u32[]{:S(2)}, u32[]{:S(2)}) collective-permute-start(bf16[64,2048]{1,0:T(8,128)(2,1)S(1)} %get-tuple-element.17), channel_id=1, source_target_pairs={{0,6},{1,7},{2,0},{3,1},{4,2},{5,3},{6,4},{7,5},{8,14},{9,15},{10,... | collective-permute-start | bytes 786440 | tf_op jit(solution)/shard_map/ppermute | solution.py:244
  129.8 2.2 %shard_map.60 = (bf16[64,2048]{1,0:T(8,128)(2,1)S(1)}, f32[64,2048]{1,0:T(8,128)S(1)}, bf16[64,2048]{1,0:T(8,128)(2,1)S(1)}, f32[64,2048]{1,0:T(8,128)S(1)}) custom-call(bf16[512,2048]{1,0:T(8,128)(2,1)S(1)} %shard_map.55.x, f32[512,2560]{1,0:T(8,128)S(1)} %shard_map.58.a, bf16[10,128,128]{2,1,0:T(8,128)(2,1)S(1)} %collective-permute-done.27.rest_0_, ...), custom_call_target="tpu_custom_call" | custom-call | flops 1845493760 | bytes 8388608 | tf_op jit(solution)/shard_map/pallas_call | solution.py:193
  132.1 0.4 collective-permute-start.32
  132.5 2.9 %collective-permute-start.36 = (bf16[64,2048]{1,0:T(8,128)(2,1)S(1)}, bf16[64,2048]{1,0:T(8,128)(2,1)S(1)}, u32[]{:S(2)}, u32[]{:S(2)}) collective-permute-start(bf16[64,2048]{1,0:T(8,128)(2,1)S(1)} %get-tuple-element.19), channel_id=1, source_target_pairs={{0,6},{1,7},{2,0},{3,1},{4,2},{5,3},{6,4},{7,5},{8,14},{9,15},{10,... | collective-permute-start | bytes 786440 | tf_op jit(solution)/shard_map/ppermute | solution.py:244
  135.4 1.5 %collective-permute-done.33.refs_1_ = bf16[64,2048]{1,0:T(8,128)(2,1)S(1)} collective-permute-done((bf16[64,2048]{1,0:T(8,128)(2,1)S(1)}, bf16[64,2048]{1,0:T(8,128)(2,1)S(1)}, u32[]{:S(2)}, u32[]{:S(2)}) %collective-permute-start.33) | collective-permute-done | bytes 262176 | tf_op jit(solution)/shard_map/ppermute | solution.py:244
  136.9 0.4 collective-permute-done.34.refs_3_
  137.3 0.1 shard_map.62
  137.4 1.7 %collective-permute-start.35 = (bf16[64,2048]{1,0:T(8,128)(2,1)S(1)}, bf16[64,2048]{1,0:T(8,128)(2,1)S(1)}, u32[]{:S(2)}, u32[]{:S(2)}) collective-permute-start(bf16[64,2048]{1,0:T(8,128)(2,1)S(1)} %get-tuple-element.18), channel_id=1, source_target_pairs={{0,2},{1,3},{2,4},{3,5},{4,6},{5,7},{6,0},{7,1},{8,10},{9,11},{10,... | collective-permute-start | bytes 786440 | tf_op jit(solution)/shard_map/ppermute | solution.py:244
  139.2 1.6 %collective-permute-start.37 = (bf16[64,2048]{1,0:T(8,128)(2,1)S(1)}, bf16[64,2048]{1,0:T(8,128)(2,1)S(1)}, u32[]{:S(2)}, u32[]{:S(2)}) collective-permute-start(bf16[64,2048]{1,0:T(8,128)(2,1)S(1)} %get-tuple-element.20), channel_id=1, source_target_pairs={{0,6},{1,7},{2,0},{3,1},{4,2},{5,3},{6,4},{7,5},{8,14},{9,15},{10,... | collective-permute-start | bytes 786440 | tf_op jit(solution)/shard_map/ppermute | solution.py:244
  140.8 1.2 shard_map.59.k
  142.0 0.6 collective-permute-done.32.f1
  142.6 0.4 collective-permute-done.36.f3
  143.0 5.0 %collective-permute-done.35.r1 = bf16[64,2048]{1,0:T(8,128)(2,1)S(1)} collective-permute-done((bf16[64,2048]{1,0:T(8,128)(2,1)S(1)}, bf16[64,2048]{1,0:T(8,128)(2,1)S(1)}, u32[]{:S(2)}, u32[]{:S(2)}) %collective-permute-start.35) | collective-permute-done | bytes 262176 | tf_op jit(solution)/shard_map/ppermute | solution.py:244
  147.9 1.5 %shard_map.63 = bf16[128,2048]{1,0:T(8,128)(2,1)} custom-call(s32[4]{0:T(128)S(1)} %pad_add_fusion.m, f32[128,2048]{1,0:T(8,128)S(1)} %shard_map.59.k, bf16[64,2048]{1,0:T(8,128)(2,1)S(1)} %collective-permute-done.32.f1, bf16[64,2048]{1,0:T(8,128)(2,1)S(1)} %collective-permute-done.35.r1, bf16[64,2048]{1,0:T(8,128)(2,1)S(1)} %collective-permute-done.36.f3, ...), custom_call_target="tpu_custom_call" | custom-call | tf_op jit(solution)/shard_map/pallas_call | solution.py:226
  (44 shorter events, 0.5 us)
Async XLA Ops:
  1.8 2.0 %collective-permute-start = (bf16[15,128,128]{2,1,0:T(8,128)(2,1)S(1)}, bf16[15,128,128]{2,1,0:T(8,128)(2,1)S(1)}, u32[]{:S(2)}, u32[]{:S(2)}) collective-permute-start(bf16[15,128,128]{2,1,0:T(8,128)(2,1)S(1)} %shard_map.56.rest_9_.rest_25_), channel_id=1, source_target_pairs={{0,1},{1,0},{2,3},{3,2},{4,5},{5,4},{6,7},{7,6},{8,9},{9,8},{10,11... | collective-permute-start | bytes 1474568 | tf_op jit(solution)/shard_map/ppermute | solution.py:247
  3.8 27.6 %collective-permute-start.1 = (bf16[10,128,128]{2,1,0:T(8,128)(2,1)S(1)}, bf16[10,128,128]{2,1,0:T(8,128)(2,1)S(1)}, u32[]{:S(2)}, u32[]{:S(2)}) collective-permute-start(bf16[10,128,128]{2,1,0:T(8,128)(2,1)S(1)} %pad_maximum_fusion.6), channel_id=1, source_target_pairs={{0,8},{1,121},{2,10},{3,123},{4,12},{5,125},{6,14},{7,127},{8,16},... | collective-permute-start | bytes 983048 | tf_op jit(solution)/shard_map/ppermute | solution.py:241
  6.7 28.1 %collective-permute-start.4 = (bf16[10,128,128]{2,1,0:T(8,128)(2,1)S(1)}, bf16[10,128,128]{2,1,0:T(8,128)(2,1)S(1)}, u32[]{:S(2)}, u32[]{:S(2)}) collective-permute-start(bf16[10,128,128]{2,1,0:T(8,128)(2,1)S(1)} %pad_maximum_fusion.7), channel_id=1, source_target_pairs={{0,8},{1,121},{2,10},{3,123},{4,12},{5,125},{6,14},{7,127},{8,16},... | collective-permute-start | bytes 983048 | tf_op jit(solution)/shard_map/ppermute | solution.py:241
  31.4 8.3 %collective-permute-start.2 = (bf16[10,128,128]{2,1,0:T(8,128)(2,1)S(1)}, bf16[10,128,128]{2,1,0:T(8,128)(2,1)S(1)}, u32[]{:S(2)}, u32[]{:S(2)}) collective-permute-start(bf16[10,128,128]{2,1,0:T(8,128)(2,1)S(1)} %collective-permute-done.1.rest_6_.rest_22_), channel_id=1, source_target_pairs={{0,8},{1,121},{2,10},{3,123},{4,12},{5,125},{6,14},{7,127},{8,16},... | collective-permute-start | bytes 983048 | tf_op jit(solution)/shard_map/ppermute | solution.py:241
  34.9 8.3 %collective-permute-start.5 = (bf16[10,128,128]{2,1,0:T(8,128)(2,1)S(1)}, bf16[10,128,128]{2,1,0:T(8,128)(2,1)S(1)}, u32[]{:S(2)}, u32[]{:S(2)}) collective-permute-start(bf16[10,128,128]{2,1,0:T(8,128)(2,1)S(1)} %collective-permute-done.4.rest_7_.rest_23_), channel_id=1, source_target_pairs={{0,8},{1,121},{2,10},{3,123},{4,12},{5,125},{6,14},{7,127},{8,16},... | collective-permute-start | bytes 983048 | tf_op jit(solution)/shard_map/ppermute | solution.py:241
  39.7 8.3 %collective-permute-start.3 = (bf16[10,128,128]{2,1,0:T(8,128)(2,1)S(1)}, bf16[10,128,128]{2,1,0:T(8,128)(2,1)S(1)}, u32[]{:S(2)}, u32[]{:S(2)}) collective-permute-start(bf16[10,128,128]{2,1,0:T(8,128)(2,1)S(1)} %collective-permute-done.2.rest_3_.rest_19_), channel_id=1, source_target_pairs={{0,8},{1,121},{2,10},{3,123},{4,12},{5,125},{6,14},{7,127},{8,16},... | collective-permute-start | bytes 983048 | tf_op jit(solution)/shard_map/ppermute | solution.py:241
  43.2 8.3 %collective-permute-start.6 = (bf16[10,128,128]{2,1,0:T(8,128)(2,1)S(1)}, bf16[10,128,128]{2,1,0:T(8,128)(2,1)S(1)}, u32[]{:S(2)}, u32[]{:S(2)}) collective-permute-start(bf16[10,128,128]{2,1,0:T(8,128)(2,1)S(1)} %collective-permute-done.5.rest_4_.rest_20_), channel_id=1, source_target_pairs={{0,8},{1,121},{2,10},{3,123},{4,12},{5,125},{6,14},{7,127},{8,16},... | collective-permute-start | bytes 983048 | tf_op jit(solution)/shard_map/ppermute | solution.py:241
  47.9 8.3 %collective-permute-start.12 = (bf16[10,128,128]{2,1,0:T(8,128)(2,1)S(1)}, bf16[10,128,128]{2,1,0:T(8,128)(2,1)S(1)}, u32[]{:S(2)}, u32[]{:S(2)}) collective-permute-start(bf16[10,128,128]{2,1,0:T(8,128)(2,1)S(1)} %collective-permute-done.3.rest_0_.rest_16_), channel_id=1, source_target_pairs={{0,8},{1,121},{2,10},{3,123},{4,12},{5,125},{6,14},{7,127},{8,16},... | collective-permute-start | bytes 983048 | tf_op jit(solution)/shard_map/ppermute | solution.py:241
  51.5 8.3 %collective-permute-start.13 = (bf16[10,128,128]{2,1,0:T(8,128)(2,1)S(1)}, bf16[10,128,128]{2,1,0:T(8,128)(2,1)S(1)}, u32[]{:S(2)}, u32[]{:S(2)}) collective-permute-start(bf16[10,128,128]{2,1,0:T(8,128)(2,1)S(1)} %collective-permute-done.6.rest_1_.rest_17_), channel_id=1, source_target_pairs={{0,8},{1,121},{2,10},{3,123},{4,12},{5,125},{6,14},{7,127},{8,16},... | collective-permute-start | bytes 983048 | tf_op jit(solution)/shard_map/ppermute | solution.py:241
  56.2 8.3 %collective-permute-start.15 = (bf16[10,128,128]{2,1,0:T(8,128)(2,1)S(1)}, bf16[10,128,128]{2,1,0:T(8,128)(2,1)S(1)}, u32[]{:S(2)}, u32[]{:S(2)}) collective-permute-start(bf16[10,128,128]{2,1,0:T(8,128)(2,1)S(1)} %collective-permute-done.12.rest_7_.rest_13_), channel_id=1, source_target_pairs={{0,8},{1,121},{2,10},{3,123},{4,12},{5,125},{6,14},{7,127},{8,16},... | collective-permute-start | bytes 983048 | tf_op jit(solution)/shard_map/ppermute | solution.py:241
  59.7 8.3 %collective-permute-start.17 = (bf16[10,128,128]{2,1,0:T(8,128)(2,1)S(1)}, bf16[10,128,128]{2,1,0:T(8,128)(2,1)S(1)}, u32[]{:S(2)}, u32[]{:S(2)}) collective-permute-start(bf16[10,128,128]{2,1,0:T(8,128)(2,1)S(1)} %collective-permute-done.13.rest_8_.rest_14_), channel_id=1, source_target_pairs={{0,8},{1,121},{2,10},{3,123},{4,12},{5,125},{6,14},{7,127},{8,16},... | collective-permute-start | bytes 983048 | tf_op jit(solution)/shard_map/ppermute | solution.py:241
  59.7 10.6 %collective-permute-start.9 = (bf16[10,128,128]{2,1,0:T(8,128)(2,1)S(1)}, bf16[10,128,128]{2,1,0:T(8,128)(2,1)S(1)}, u32[]{:S(2)}, u32[]{:S(2)}) collective-permute-start(bf16[10,128,128]{2,1,0:T(8,128)(2,1)S(1)} %collective-permute-done.1.rest_6_.rest_22_), channel_id=1, source_target_pairs={{0,128},{128,0},{1,129},{129,1},{2,130},{130,2},{3,131},{131,3},{4... | collective-permute-start | bytes 983048 | tf_op jit(solution)/shard_map/ppermute | solution.py:250
  59.8 16.5 %collective-permute-start.8 = (bf16[10,128,128]{2,1,0:T(8,128)(2,1)S(1)}, bf16[10,128,128]{2,1,0:T(8,128)(2,1)S(1)}, u32[]{:S(2)}, u32[]{:S(2)}) collective-permute-start(bf16[10,128,128]{2,1,0:T(8,128)(2,1)S(1)} %collective-permute-done.2.rest_3_.rest_19_), channel_id=1, source_target_pairs={{0,128},{128,0},{1,129},{129,1},{2,130},{130,2},{3,131},{131,3},{4... | collective-permute-start | bytes 983048 | tf_op jit(solution)/shard_map/ppermute | solution.py:250
  64.5 8.3 %collective-permute-start.16 = (bf16[10,128,128]{2,1,0:T(8,128)(2,1)S(1)}, bf16[10,128,128]{2,1,0:T(8,128)(2,1)S(1)}, u32[]{:S(2)}, u32[]{:S(2)}) collective-permute-start(bf16[10,128,128]{2,1,0:T(8,128)(2,1)S(1)} %collective-permute-done.15.rest_4_.rest_10_), channel_id=1, source_target_pairs={{0,8},{1,121},{2,10},{3,123},{4,12},{5,125},{6,14},{7,127},{8,16},... | collective-permute-start | bytes 983048 | tf_op jit(solution)/shard_map/ppermute | solution.py:241
  68.0 8.3 %collective-permute-start.18 = (bf16[10,128,128]{2,1,0:T(8,128)(2,1)S(1)}, bf16[10,128,128]{2,1,0:T(8,128)(2,1)S(1)}, u32[]{:S(2)}, u32[]{:S(2)}) collective-permute-start(bf16[10,128,128]{2,1,0:T(8,128)(2,1)S(1)} %collective-permute-done.17.rest_5_.rest_11_), channel_id=1, source_target_pairs={{0,8},{1,121},{2,10},{3,123},{4,12},{5,125},{6,14},{7,127},{8,16},... | collective-permute-start | bytes 983048 | tf_op jit(solution)/shard_map/ppermute | solution.py:241
  70.5 41.3 %collective-permute-start.10 = (bf16[50,128,128]{2,1,0:T(8,128)(2,1)S(1)}, bf16[50,128,128]{2,1,0:T(8,128)(2,1)S(1)}, u32[]{:S(2)}, u32[]{:S(2)}) collective-permute-start(bf16[50,128,128]{2,1,0:T(8,128)(2,1)S(1)} %constant_dynamic-update-slice_fusion), channel_id=1, source_target_pairs={{0,1},{1,0},{2,3},{3,2},{4,5},{5,4},{6,7},{7,6},{8,9},{9,8},{10,11... | collective-permute-start | bytes 4915208 | tf_op jit(solution)/shard_map/ppermute | solution.py:247
  70.8 11.1 %collective-permute-start.7 = (bf16[10,128,128]{2,1,0:T(8,128)(2,1)S(1)}, bf16[10,128,128]{2,1,0:T(8,128)(2,1)S(1)}, u32[]{:S(2)}, u32[]{:S(2)}) collective-permute-start(bf16[10,128,128]{2,1,0:T(8,128)(2,1)S(1)} %collective-permute-done.3.rest_0_.rest_16_), channel_id=1, source_target_pairs={{0,128},{128,0},{1,129},{129,1},{2,130},{130,2},{3,131},{131,3},{4... | collective-permute-start | bytes 983048 | tf_op jit(solution)/shard_map/ppermute | solution.py:250
  72.8 9.4 %collective-permute-start.24 = (bf16[10,128,128]{2,1,0:T(8,128)(2,1)S(1)}, bf16[10,128,128]{2,1,0:T(8,128)(2,1)S(1)}, u32[]{:S(2)}, u32[]{:S(2)}) collective-permute-start(bf16[10,128,128]{2,1,0:T(8,128)(2,1)S(1)} %collective-permute-done.16.rest_1_.rest_7_), channel_id=1, source_target_pairs={{0,8},{1,121},{2,10},{3,123},{4,12},{5,125},{6,14},{7,127},{8,16},... | collective-permute-start | bytes 983048 | tf_op jit(solution)/shard_map/ppermute | solution.py:241
  76.3 8.3 %collective-permute-start.25 = (bf16[10,128,128]{2,1,0:T(8,128)(2,1)S(1)}, bf16[10,128,128]{2,1,0:T(8,128)(2,1)S(1)}, u32[]{:S(2)}, u32[]{:S(2)}) collective-permute-start(bf16[10,128,128]{2,1,0:T(8,128)(2,1)S(1)} %collective-permute-done.18.rest_2_.rest_8_), channel_id=1, source_target_pairs={{0,8},{1,121},{2,10},{3,123},{4,12},{5,125},{6,14},{7,127},{8,16},... | collective-permute-start | bytes 983048 | tf_op jit(solution)/shard_map/ppermute | solution.py:241
  76.4 30.3 %collective-permute-start.11 = (bf16[30,128,128]{2,1,0:T(8,128)(2,1)S(1)}, bf16[30,128,128]{2,1,0:T(8,128)(2,1)S(1)}, u32[]{:S(2)}, u32[]{:S(2)}) collective-permute-start(bf16[30,128,128]{2,1,0:T(8,128)(2,1)S(1)} %pad_maximum_fusion), channel_id=1, source_target_pairs={{0,1},{1,0},{2,3},{3,2},{4,5},{5,4},{6,7},{7,6},{8,9},{9,8},{10,11... | collective-permute-start | bytes 2949128 | tf_op jit(solution)/shard_map/ppermute | solution.py:247
  81.9 10.6 %collective-permute-start.21 = (bf16[10,128,128]{2,1,0:T(8,128)(2,1)S(1)}, bf16[10,128,128]{2,1,0:T(8,128)(2,1)S(1)}, u32[]{:S(2)}, u32[]{:S(2)}) collective-permute-start(bf16[10,128,128]{2,1,0:T(8,128)(2,1)S(1)} %collective-permute-done.12.rest_7_.rest_13_), channel_id=1, source_target_pairs={{0,128},{128,0},{1,129},{129,1},{2,130},{130,2},{3,131},{131,3},{4... | collective-permute-start | bytes 983048 | tf_op jit(solution)/shard_map/ppermute | solution.py:250
  82.2 17.3 %collective-permute-start.20 = (bf16[10,128,128]{2,1,0:T(8,128)(2,1)S(1)}, bf16[10,128,128]{2,1,0:T(8,128)(2,1)S(1)}, u32[]{:S(2)}, u32[]{:S(2)}) collective-permute-start(bf16[10,128,128]{2,1,0:T(8,128)(2,1)S(1)} %collective-permute-done.15.rest_4_.rest_10_), channel_id=1, source_target_pairs={{0,128},{128,0},{1,129},{129,1},{2,130},{130,2},{3,131},{131,3},{4... | collective-permute-start | bytes 983048 | tf_op jit(solution)/shard_map/ppermute | solution.py:250
  84.6 21.9 %collective-permute-start.19 = (bf16[10,128,128]{2,1,0:T(8,128)(2,1)S(1)}, bf16[10,128,128]{2,1,0:T(8,128)(2,1)S(1)}, u32[]{:S(2)}, u32[]{:S(2)}) collective-permute-start(bf16[10,128,128]{2,1,0:T(8,128)(2,1)S(1)} %collective-permute-done.16.rest_1_.rest_7_), channel_id=1, source_target_pairs={{0,128},{128,0},{1,129},{129,1},{2,130},{130,2},{3,131},{131,3},{4... | collective-permute-start | bytes 983048 | tf_op jit(solution)/shard_map/ppermute | solution.py:250
  92.5 14.9 %collective-permute-start.27 = (bf16[10,128,128]{2,1,0:T(8,128)(2,1)S(1)}, bf16[10,128,128]{2,1,0:T(8,128)(2,1)S(1)}, u32[]{:S(2)}, u32[]{:S(2)}) collective-permute-start(bf16[10,128,128]{2,1,0:T(8,128)(2,1)S(1)} %pad_maximum_fusion.8), channel_id=1, source_target_pairs={{0,8},{1,121},{2,10},{3,123},{4,12},{5,125},{6,14},{7,127},{8,16},... | collective-permute-start | bytes 983048 | tf_op jit(solution)/shard_map/ppermute | solution.py:241
  99.5 12.2 %collective-permute-start.28 = (bf16[10,128,128]{2,1,0:T(8,128)(2,1)S(1)}, bf16[10,128,128]{2,1,0:T(8,128)(2,1)S(1)}, u32[]{:S(2)}, u32[]{:S(2)}) collective-permute-start(bf16[10,128,128]{2,1,0:T(8,128)(2,1)S(1)} %collective-permute-done.24.rest_4_), channel_id=1, source_target_pairs={{0,128},{128,0},{1,129},{129,1},{2,130},{130,2},{3,131},{131,3},{4... | collective-permute-start | bytes 983048 | tf_op jit(solution)/shard_map/ppermute | solution.py:250
  106.5 9.6 %collective-permute-start.14 = (bf16[30,128,128]{2,1,0:T(8,128)(2,1)S(1)}, bf16[30,128,128]{2,1,0:T(8,128)(2,1)S(1)}, u32[]{:S(2)}, u32[]{:S(2)}) collective-permute-start(bf16[30,128,128]{2,1,0:T(8,128)(2,1)S(1)} %pad_maximum_fusion.1), channel_id=1, source_target_pairs={{0,1},{1,0},{2,3},{3,2},{4,5},{5,4},{6,7},{7,6},{8,9},{9,8},{10,11... | collective-permute-start | bytes 2949128 | tf_op jit(solution)/shard_map/ppermute | solution.py:247
  106.6 5.8 %copy-start = (bf16[2048]{0:T(1024)(128)(2,1)S(1)}, bf16[2048]{0:T(1024)(128)(2,1)}, u32[]{:S(2)}) copy-start(bf16[2048]{0:T(1024)(128)(2,1)} %param.6) | copy-start | bytes 12292
  106.8 15.9 %collective-permute-start.22 = (bf16[30,128,128]{2,1,0:T(8,128)(2,1)S(1)}, bf16[30,128,128]{2,1,0:T(8,128)(2,1)S(1)}, u32[]{:S(2)}, u32[]{:S(2)}) collective-permute-start(bf16[30,128,128]{2,1,0:T(8,128)(2,1)S(1)} %pad_maximum_fusion.2), channel_id=1, source_target_pairs={{0,1},{1,0},{2,3},{3,2},{4,5},{5,4},{6,7},{7,6},{8,9},{9,8},{10,11... | collective-permute-start | bytes 2949128 | tf_op jit(solution)/shard_map/ppermute | solution.py:247
  107.4 15.3 %collective-permute-start.23 = (bf16[30,128,128]{2,1,0:T(8,128)(2,1)S(1)}, bf16[30,128,128]{2,1,0:T(8,128)(2,1)S(1)}, u32[]{:S(2)}, u32[]{:S(2)}) collective-permute-start(bf16[30,128,128]{2,1,0:T(8,128)(2,1)S(1)} %pad_maximum_fusion.3), channel_id=1, source_target_pairs={{0,1},{1,0},{2,3},{3,2},{4,5},{5,4},{6,7},{7,6},{8,9},{9,8},{10,11... | collective-permute-start | bytes 2949128 | tf_op jit(solution)/shard_map/ppermute | solution.py:247
  111.7 11.0 %collective-permute-start.26 = (bf16[30,128,128]{2,1,0:T(8,128)(2,1)S(1)}, bf16[30,128,128]{2,1,0:T(8,128)(2,1)S(1)}, u32[]{:S(2)}, u32[]{:S(2)}) collective-permute-start(bf16[30,128,128]{2,1,0:T(8,128)(2,1)S(1)} %pad_maximum_fusion.4), channel_id=1, source_target_pairs={{0,1},{1,0},{2,3},{3,2},{4,5},{5,4},{6,7},{7,6},{8,9},{9,8},{10,11... | collective-permute-start | bytes 2949128 | tf_op jit(solution)/shard_map/ppermute | solution.py:247
  111.8 13.4 %collective-permute-start.29 = (bf16[20,128,128]{2,1,0:T(8,128)(2,1)S(1)}, bf16[20,128,128]{2,1,0:T(8,128)(2,1)S(1)}, u32[]{:S(2)}, u32[]{:S(2)}) collective-permute-start(bf16[20,128,128]{2,1,0:T(8,128)(2,1)S(1)} %pad_maximum_fusion.5), channel_id=1, source_target_pairs={{0,1},{1,0},{2,3},{3,2},{4,5},{5,4},{6,7},{7,6},{8,9},{9,8},{10,11... | collective-permute-start | bytes 1966088 | tf_op jit(solution)/shard_map/ppermute | solution.py:247
  116.2 6.5 %collective-permute-start.30 = (bf16[5,128,128]{2,1,0:T(8,128)(2,1)S(1)}, bf16[5,128,128]{2,1,0:T(8,128)(2,1)S(1)}, u32[]{:S(2)}, u32[]{:S(2)}) collective-permute-start(bf16[5,128,128]{2,1,0:T(8,128)(2,1)S(1)} %slice.34), channel_id=1, source_target_pairs={{0,128},{128,0},{1,129},{129,1},{2,130},{130,2},{3,131},{131,3},{4... | collective-permute-start | bytes 491528 | tf_op jit(solution)/shard_map/ppermute | solution.py:250
  122.7 2.5 %collective-permute-start.31 = (bf16[5,128,128]{2,1,0:T(8,128)(2,1)S(1)}, bf16[5,128,128]{2,1,0:T(8,128)(2,1)S(1)}, u32[]{:S(2)}, u32[]{:S(2)}) collective-permute-start(bf16[5,128,128]{2,1,0:T(8,128)(2,1)S(1)} %collective-permute-done.30.rest_2_), channel_id=1, source_target_pairs={{0,1},{1,0},{2,3},{3,2},{4,5},{5,4},{6,7},{7,6},{8,9},{9,8},{10,11... | collective-permute-start | bytes 491528 | tf_op jit(solution)/shard_map/ppermute | solution.py:247
  126.4 10.5 %collective-permute-start.33 = (bf16[64,2048]{1,0:T(8,128)(2,1)S(1)}, bf16[64,2048]{1,0:T(8,128)(2,1)S(1)}, u32[]{:S(2)}, u32[]{:S(2)}) collective-permute-start(bf16[64,2048]{1,0:T(8,128)(2,1)S(1)} %get-tuple-element.15), channel_id=1, source_target_pairs={{0,2},{1,3},{2,4},{3,5},{4,6},{5,7},{6,0},{7,1},{8,10},{9,11},{10,... | collective-permute-start | bytes 786440 | tf_op jit(solution)/shard_map/ppermute | solution.py:244
  128.2 9.2 %collective-permute-start.34 = (bf16[64,2048]{1,0:T(8,128)(2,1)S(1)}, bf16[64,2048]{1,0:T(8,128)(2,1)S(1)}, u32[]{:S(2)}, u32[]{:S(2)}) collective-permute-start(bf16[64,2048]{1,0:T(8,128)(2,1)S(1)} %get-tuple-element.17), channel_id=1, source_target_pairs={{0,6},{1,7},{2,0},{3,1},{4,2},{5,3},{6,4},{7,5},{8,14},{9,15},{10,... | collective-permute-start | bytes 786440 | tf_op jit(solution)/shard_map/ppermute | solution.py:244
  132.1 10.5 %collective-permute-start.32 = (bf16[64,2048]{1,0:T(8,128)(2,1)S(1)}, bf16[64,2048]{1,0:T(8,128)(2,1)S(1)}, u32[]{:S(2)}, u32[]{:S(2)}) collective-permute-start(bf16[64,2048]{1,0:T(8,128)(2,1)S(1)} %get-tuple-element.13), channel_id=1, source_target_pairs={{0,2},{1,3},{2,4},{3,5},{4,6},{5,7},{6,0},{7,1},{8,10},{9,11},{10,... | collective-permute-start | bytes 786440 | tf_op jit(solution)/shard_map/ppermute | solution.py:244
  132.5 10.4 %collective-permute-start.36 = (bf16[64,2048]{1,0:T(8,128)(2,1)S(1)}, bf16[64,2048]{1,0:T(8,128)(2,1)S(1)}, u32[]{:S(2)}, u32[]{:S(2)}) collective-permute-start(bf16[64,2048]{1,0:T(8,128)(2,1)S(1)} %get-tuple-element.19), channel_id=1, source_target_pairs={{0,6},{1,7},{2,0},{3,1},{4,2},{5,3},{6,4},{7,5},{8,14},{9,15},{10,... | collective-permute-start | bytes 786440 | tf_op jit(solution)/shard_map/ppermute | solution.py:244
  137.4 10.5 %collective-permute-start.35 = (bf16[64,2048]{1,0:T(8,128)(2,1)S(1)}, bf16[64,2048]{1,0:T(8,128)(2,1)S(1)}, u32[]{:S(2)}, u32[]{:S(2)}) collective-permute-start(bf16[64,2048]{1,0:T(8,128)(2,1)S(1)} %get-tuple-element.18), channel_id=1, source_target_pairs={{0,2},{1,3},{2,4},{3,5},{4,6},{5,7},{6,0},{7,1},{8,10},{9,11},{10,... | collective-permute-start | bytes 786440 | tf_op jit(solution)/shard_map/ppermute | solution.py:244
  139.2 8.8 %collective-permute-start.37 = (bf16[64,2048]{1,0:T(8,128)(2,1)S(1)}, bf16[64,2048]{1,0:T(8,128)(2,1)S(1)}, u32[]{:S(2)}, u32[]{:S(2)}) collective-permute-start(bf16[64,2048]{1,0:T(8,128)(2,1)S(1)} %get-tuple-element.20), channel_id=1, source_target_pairs={{0,6},{1,7},{2,0},{3,1},{4,2},{5,3},{6,4},{7,5},{8,14},{9,15},{10,... | collective-permute-start | bytes 786440 | tf_op jit(solution)/shard_map/ppermute | solution.py:244
